TPU v7x, 32 devices: a whole 2x2x4 slice. The times are simulated.
32 devices in a mesh: grp: 2 (over y), ep: 4 (over z), tp: 4 (over x, core).
Axes of the slice: x: 2, y: 2, z: 4, core: 2. Of those that a mesh axis runs over, the one named last changes fastest.
Arguments:
- queries: bfloat16 [3072, 1024], P(('grp', 'ep'), 'tp'), parts along dimension 0, may hold values from -6 to 6
- key_values: bfloat16 [3072, 512], P(('grp', 'ep'), 'tp'), parts along dimension 0, may hold values from -6 to 6
- query_gain: float32 [64], replicated, may hold values from 0.5 to 5
- key_gain: float32 [64], replicated, may hold values from 0.5 to 5
- out_weight: bfloat16 [1024, 2048], P('tp'), may hold values from -0.1875 to 0.1875
- second_batch: bfloat16 [4096, 2048], P(('grp', 'ep', 'tp')), parts along dimension 0, may hold values from -6 to 6
- norm_gain: float32 [2048], replicated, may hold values from 0.1 to 1.9
- routes: int32 [4096, 2], P(('grp', 'ep', 'tp')), parts along dimension 0, may hold values from 0 to 7, all different within a row; in each aligned block of 128 rows (0 to 127, 128 to 255, ...) at most 48 rows name the same one
- route_weights: float32 [4096, 2], P(('grp', 'ep', 'tp')), parts along dimension 0, may hold values from 0.2 to 1
- expert_gate: bfloat16 [8, 2048, 1024], P('ep', None, 'tp'), may hold values from -0.125 to 0.125
- expert_up: bfloat16 [8, 2048, 1024], P('ep', None, 'tp'), may hold values from -0.125 to 0.125
- expert_down: bfloat16 [8, 1024, 2048], P('ep', 'tp'), may hold values from -0.1875 to 0.1875
- shared_gate: bfloat16 [2048, 512], P(None, 'tp'), may hold values from -0.125 to 0.125
- shared_up: bfloat16 [2048, 512], P(None, 'tp'), may hold values from -0.125 to 0.125
- shared_down: bfloat16 [512, 2048], P('tp'), may hold values from -0.25 to 0.25
Outputs:
- mixer_out: bfloat16 [3072, 2048], P(('grp', 'ep', 'tp')), parts along dimension 0
- channel_out: bfloat16 [4096, 2048], P(('grp', 'ep', 'tp')), parts along dimension 0
There are 2 independent parts, one for each index of `grp`. A program takes and returns all parts, laid end to end along the dimension named above; an argument that names none is the same for every part. Nothing has to cross between parts.
Inputs may be any that keep to these rules, and one draw needn't show every extreme that they name: `routes`: each row names 2 different experts. Among the rows of one device no expert is named more than 48 times, and in every draw some expert is named exactly 48 times by the rows of some device.
All inputs are finite; a program needn't handle non-finite values.
Results may differ from a plain program's by a relative error of at most 0.015.
The roundings to bfloat16 on the way count: a program that leaves them out, or rounds other values in their place, can miss the bound.
Values may be sent and summed in bfloat16 or wider, within the bound.
A program may use at most 128 MiB of HBM per device.

v0:
```python
import jax
import jax.numpy as jnp
from jax import lax
from jax.sharding import PartitionSpec as P

GRID_W = 64


rope_base = 10000.0
norm_eps = 1e-06


def head_norm(vectors, gain):
    return (
        vectors * lax.rsqrt(jnp.mean(vectors * vectors, axis=-1, keepdims=True) + norm_eps) * gain
    )


def turn_heads(vectors, positions):
    row_count, head_count, head_size = vectors.shape
    half_size = head_size // 2
    inverse = rope_base ** (-jnp.arange(0, half_size, 2, dtype=jnp.float32) / half_size)
    grid_row = (positions // GRID_W).astype(jnp.float32)
    grid_column = (positions % GRID_W).astype(jnp.float32)
    angles = jnp.concatenate([grid_row[:, None] * inverse, grid_column[:, None] * inverse], axis=-1)
    cosine = jnp.cos(angles)[:, None, :]
    sine = jnp.sin(angles)[:, None, :]
    paired = vectors.reshape(row_count, head_count, half_size, 2)
    first = paired[..., 0]
    second = paired[..., 1]
    turned = jnp.stack([first * cosine - second * sine, first * sine + second * cosine], axis=-1)
    return turned.reshape(vectors.shape)


def slot_ids(route_rows, expert_count, capacity):
    row_count, top_count = route_rows.shape
    flat_routes = route_rows.reshape(-1)
    onehot = (flat_routes[:, None] == jnp.arange(expert_count, dtype=jnp.int32)[None, :]).astype(
        jnp.int32
    )
    earlier = jnp.cumsum(onehot, axis=0) - onehot
    within = jnp.sum(earlier * onehot, axis=1)
    return (flat_routes * capacity + within).reshape(row_count, top_count)


def slot_table(slots, slot_count):
    row_count, top_count = slots.shape
    flat_slots = slots.reshape(-1)
    owner_row = jnp.arange(row_count * top_count, dtype=jnp.int32) // top_count
    matches = flat_slots[None, :] == jnp.arange(slot_count, dtype=jnp.int32)[:, None]
    occupied = jnp.any(matches, axis=1)
    source_row = jnp.sum(jnp.where(matches, owner_row[None, :], 0), axis=1)
    return jnp.where(occupied, source_row, row_count)


def pick_block(row_count):
    for candidate in range(min(row_count, 1024), 0, -1):
        if row_count % candidate == 0:
            return candidate
    return row_count


def attend_keys(query_turned, scale, running, pieces):
    head_size = query_turned.shape[-1]
    key_block = pick_block(pieces.shape[0])
    blocks = pieces.reshape(pieces.shape[0] // key_block, key_block, 2 * head_size)

    def one_block(carried, block_rows):
        top_now, total_now, acc_now = carried
        scores = (
            jnp.einsum(
                "qhd,kd->hqk",
                query_turned,
                block_rows[:, :head_size],
                preferred_element_type=jnp.float32,
            )
            * scale
        )
        top_new = jnp.maximum(top_now, jnp.max(scores, axis=-1))
        shrink = jnp.exp(top_now - top_new)
        exps = jnp.exp(scores - top_new[..., None])
        total_new = total_now * shrink + jnp.sum(exps, axis=-1)
        acc_new = acc_now * shrink[..., None] + jnp.einsum(
            "hqk,kd->hqd",
            exps.astype(jnp.bfloat16),
            block_rows[:, head_size:],
            preferred_element_type=jnp.float32,
        )
        return ((top_new, total_new, acc_new), None)

    result, ignored = lax.scan(one_block, running, blocks)
    return result


def shared_hidden_of(token_rows, gate_weights, up_weights):
    gate_part = jnp.dot(token_rows, gate_weights, preferred_element_type=jnp.float32)
    up_part = jnp.dot(token_rows, up_weights, preferred_element_type=jnp.float32)
    return (jax.nn.silu(gate_part) * up_part).astype(jnp.bfloat16)


def expert_hidden(slot_rows, gate_weights, up_weights):
    gate_part = jnp.einsum(
        "osjcd,jdf->osjcf", slot_rows, gate_weights, preferred_element_type=jnp.float32
    )
    up_part = jnp.einsum(
        "osjcd,jdf->osjcf", slot_rows, up_weights, preferred_element_type=jnp.float32
    )
    return (jax.nn.silu(gate_part) * up_part).astype(jnp.bfloat16)


def body(
    queries,
    key_values,
    query_gain,
    key_gain,
    out_weight,
    second_batch,
    norm_gain,
    routes,
    route_weights,
    expert_gate,
    expert_up,
    expert_down,
    shared_gate,
    shared_up,
    shared_down,
):
    query_rows = queries.shape[0]
    head_size = query_gain.shape[0]
    heads_here = queries.shape[1] // head_size
    ep_count = lax.axis_size("ep")
    positions = lax.axis_index("ep") * query_rows + jnp.arange(query_rows, dtype=jnp.int32)
    query_turned = turn_heads(
        head_norm(
            queries.reshape(query_rows, heads_here, head_size).astype(jnp.float32), query_gain
        ),
        positions,
    ).astype(jnp.bfloat16)
    key_turned = turn_heads(
        head_norm(key_values[:, None, :head_size].astype(jnp.float32), key_gain), positions
    ).astype(jnp.bfloat16)
    keys_and_values = jnp.concatenate([key_turned[:, 0, :], key_values[:, head_size:]], axis=1)
    start_state = (
        jnp.full((heads_here, query_rows), -1e30, jnp.float32),
        jnp.zeros((heads_here, query_rows), jnp.float32),
        jnp.zeros((heads_here, query_rows, head_size), jnp.float32),
    )
    top_all, total_all, acc_all = attend_keys(
        query_turned,
        head_size ** (-0.5),
        start_state,
        lax.all_gather(keys_and_values, "ep", axis=0, tiled=True),
    )
    head_out = (
        (acc_all / total_all[..., None])
        .transpose(1, 0, 2)
        .reshape(query_rows, heads_here * head_size)
        .astype(jnp.bfloat16)
    )
    tok_count = second_batch.shape[0]
    model_width = second_batch.shape[1]
    top_count = routes.shape[1]
    local_experts = expert_gate.shape[0]
    expert_count = local_experts * ep_count
    capacity = 3 * tok_count * top_count // (2 * expert_count)
    slot_count = expert_count * capacity
    token_float = second_batch.astype(jnp.float32)
    normed = (
        token_float
        * lax.rsqrt(jnp.mean(token_float * token_float, axis=-1, keepdims=True) + norm_eps)
        * norm_gain
    ).astype(jnp.bfloat16)
    own_slots = slot_ids(routes, expert_count, capacity)
    shared_hidden = shared_hidden_of(
        lax.all_gather(normed, "tp", axis=0, tiled=True), shared_gate, shared_up
    )
    outgoing = jnp.take(
        normed, slot_table(own_slots, slot_count), axis=0, mode="fill", fill_value=0
    )[None]
    arrived = lax.all_to_all(outgoing, "ep", split_axis=1, concat_axis=1, tiled=True)
    arrived = arrived.reshape(arrived.shape[0], ep_count, local_experts, capacity, model_width)
    hidden = expert_hidden(
        lax.all_gather(arrived, "tp", axis=0, tiled=True), expert_gate, expert_up
    )
    routed_part = jnp.einsum(
        "osjcf,jfd->osjcd", hidden, expert_down, preferred_element_type=jnp.float32
    ).reshape(-1, model_width)
    shared_part = jnp.dot(shared_hidden, shared_down, preferred_element_type=jnp.float32)
    head_partial = jnp.dot(head_out, out_weight, preferred_element_type=jnp.float32)
    attn_sum, routed_sum, shared_sum = (
        lax.psum_scatter(
            head_partial.astype(jnp.bfloat16), "tp", scatter_dimension=0, tiled=True
        ).astype(jnp.float32),
        lax.psum_scatter(
            routed_part.astype(jnp.bfloat16), "tp", scatter_dimension=0, tiled=True
        ).astype(jnp.float32),
        lax.psum_scatter(
            shared_part.astype(jnp.bfloat16), "tp", scatter_dimension=0, tiled=True
        ).astype(jnp.float32),
    )
    returned = lax.all_to_all(
        routed_sum.astype(jnp.bfloat16), "ep", split_axis=0, concat_axis=0, tiled=True
    )
    combined = shared_sum
    for slot_pick in range(top_count):
        combined = combined + route_weights[:, slot_pick : slot_pick + 1] * jnp.take(
            returned, own_slots[:, slot_pick], axis=0
        ).astype(jnp.float32)
    return (attn_sum.astype(jnp.bfloat16), combined.astype(jnp.bfloat16))


def solution(mesh):
    placed = (
        P(("grp", "ep"), "tp"),
        P(("grp", "ep"), "tp"),
        P(),
        P(),
        P("tp", None),
        P(("grp", "ep", "tp"), None),
        P(),
        P(("grp", "ep", "tp"), None),
        P(("grp", "ep", "tp"), None),
        P("ep", None, "tp"),
        P("ep", None, "tp"),
        P("ep", "tp", None),
        P(None, "tp"),
        P(None, "tp"),
        P("tp", None),
    )
    return jax.shard_map(
        body,
        mesh=mesh,
        in_specs=placed,
        out_specs=(P(("grp", "ep", "tp"), None), P(("grp", "ep", "tp"), None)),
        check_vma=False,
    )
```

profile of v0, /device:TPU:0, one launch (start us, length us, event | category | flops | bytes accessed | tf_op | source)
XLA Modules:
  0.0 293.0 jit_solution(5934166044517611856)
XLA Ops:
  12.2 3.1 %gather_fusion = bf16[384,2048]{1,0:T(8,128)(2,1)} fusion(bf16[128,2048]{1,0:T(8,128)(2,1)S(1)} %fusion.27, s32[1024]{0:T(1024)S(1)} %pad_clamp_fusion.2), kind=kCustom, calls=%fused_computation.2 | custom fusion | bytes 3147264 | tf_op jit(solution)/shard_map/jit(_take)/gather | solution.py:177
  17.0 4.1 %copy.106 = bf16[1,384,2048]{2,0,1:T(2,128)(2,1)} copy(bf16[1,384,2048]{2,1,0:T(8,128)(2,1)S(1)} %bitcast_select_fusion) | data formatting | bytes 3145728 | tf_op jit(solution)/shard_map/jit(_take)/select_n | solution.py:177
  21.5 12.4 %reduce.6 = bf16[384,2048]{1,0:T(8,128)(2,1)} reduce(bf16[384,1,2048]{2,1,0:T(2,128)(2,1)} %bitcast.138, bf16[]{:T(256)} %broadcast.414), dimensions={1}, to_apply=%bitcast.118.reduce_sub_computation | reduce | bytes 3145730
  33.9 4.1 %reshape.479 = bf16[4,2,98304]{2,1,0:T(2,128)(2,1)} reshape(bf16[384,2048]{1,0:T(8,128)(2,1)} %reduce.6) | data formatting | bytes 3145728
  38.0 43.4 %all_to_all.17 = bf16[4,2,98304]{2,1,0:T(2,128)(2,1)} all-to-all(bf16[4,2,98304]{2,1,0:T(2,128)(2,1)} %reshape.479), channel_id=1, replica_groups=mesh['grp'=2,'ep'=4,'tp'=4] {'ep'}, dimensions={0} | all-to-all | bytes 3145728 | tf_op jit(solution)/shard_map/all_to_all | solution.py:180
  81.4 4.5 %reshape.480 = bf16[384,1,2048]{2,1,0:T(2,128)(2,1)} reshape(bf16[4,2,98304]{2,1,0:T(2,128)(2,1)} %all_to_all.17) | data formatting | bytes 3145728
  85.9 2.8 copy.96
  90.9 44.9 %all-gather.5.cloned.1.call-done = bf16[4,4,2,48,2048]{4,3,1,0,2:T(8,128)(2,1)} async-done(((bf16[1,4,2,48,2048]{4,3,1,0,2:T(8,128)(2,1)}), bf16[4,4,2,48,2048]{4,3,1,0,2:T(8,128)(2,1)}) %all-gather.5.cloned.1.call-update) | async-done | bytes 6291472 | tf_op jit(solution)/shard_map/all_gather | solution.py:183
  135.7 6.4 %fusion.14 = f32[2,4,4,48,256]{4,3,2,1,0:T(8,128)} fusion(bf16[4,4,2,48,2048]{4,3,1,0,2:T(8,128)(2,1)} %all-gather.5.cloned.1.call-done, bf16[2,2048,256]{2,1,0:T(8,128)(2,1)} %param.28), kind=kOutput, calls=%fused_computation.26 | convolution fusion | flops 1610612736 | bytes 9961472 | tf_op jit(solution)/shard_map/osjcd,jdf->osjcf/dot_general | solution.py:102
  142.1 10.7 %convert_bitcast_fusion = bf16[4,4,2,48,2048]{4,3,1,0,2:T(8,128)(2,1)} fusion(bf16[2,256,2048]{2,1,0:T(8,128)(2,1)S(1)} %copy-done, f32[2,4,4,48,256]{4,3,2,1,0:T(8,128)} %fusion.14, bf16[4,4,2,48,2048]{4,3,1,0,2:T(8,128)(2,1)} %all-gather.5.cloned.1.call-done, bf16[2,2048,256]{2,1,0:T(8,128)(2,1)} %param.29), kind=kOutput, calls=%fused_computation.20 | convolution fusion | flops 3226730496 | bytes 18350080 | tf_op jit(solution)/shard_map/osjcf,jfd->osjcd/dot_general | solution.py:185
  152.9 6.6 %copy.90 = bf16[4,4,2,48,2048]{4,3,2,1,0:T(8,128)(2,1)} copy(bf16[4,4,2,48,2048]{4,3,1,0,2:T(8,128)(2,1)} %convert_bitcast_fusion) | data formatting | bytes 12582912 | tf_op jit(solution)/shard_map/convert_element_type | solution.py:195
  162.7 2.4 fusion.57
  165.2 4.9 %convolution_convert_fusion = bf16[512,2048]{1,0:T(8,128)(2,1)} fusion(bf16[128,2048]{1,0:T(8,128)(2,1)} %param.33, bf16[512,2048]{1,0:T(8,128)(2,1)S(1)} %copy-done.5, bf16[2048,128]{1,0:T(8,128)(2,1)} %param.32, f32[512,128]{1,0:T(8,128)S(1)} %fusion.57), kind=kOutput, calls=%fused_computation.21 | convolution fusion | flops 538312704 | bytes 5505024 | tf_op jit(solution)/shard_map/dot_general | solution.py:188
  171.1 14.6 %all_gather.9 = bf16[1536,128]{0,1:T(8,128)(2,1)S(1)} all-gather(bf16[384,128]{0,1:T(8,128)(2,1)S(1)} %pad_maximum_fusion.1), channel_id=1, replica_groups=mesh['grp'=2,'ep'=4,'tp'=4] {'ep'}, dimensions={0}, use_global_device_ids=true | all-gather | bytes 491520 | tf_op jit(solution)/shard_map/all_gather | solution.py:152
  185.9 15.9 %while.15 = (s32[]{:T(128)}, f32[4,384]{1,0:T(4,128)S(1)}, f32[4,384]{1,0:T(4,128)S(1)}, f32[4,384,64]{1,2,0:T(8,128)S(1)}, bf16[2,768,128]{2,1,0:T(8,128)(2,1)S...) while((s32[]{:T(128)}, f32[4,384]{1,0:T(4,128)S(1)}, f32[4,384]{1,0:T(4,128)S(1)}, ...), condition=%wide.region_5.6_spmd.clone, body=%wide.region_2.5_spmd.clone.sunk | while | flops 311729664 | bytes 35094656 | solution.py:91
  186.1 3.0 %bitcast_reduce_fusion.3 = (f32[4,384]{1,0:T(4,128)S(1)}, f32[768,384,4]{1,0,2:T(8,128)}) fusion(bf16[384,4,64]{0,2,1:T(8,128)(2,1)S(1)} %get-tuple-element.203, bf16[768,128]{0,1:T(8,128)(2,1)S(1)} %bitcast.136), kind=kOutput, calls=%fused_computation.4.clone.1 | convolution fusion | flops 153352704 | bytes 5019648 | tf_op jit(solution)/shard_map/while/body/eval_jaxpr/qhd,kd->hqk/dot_general | solution.py:71
  189.1 3.3 %fusion.75 = f32[4,384]{1,0:T(4,128)S(1)} fusion(f32[768,384,4]{1,0,2:T(8,128)} %get-tuple-element.179, f32[4,384]{1,0:T(4,128)S(1)} %select_maximum_fusion.2), kind=kLoop, calls=%fused_computation.7.clone.1 | loop fusion | flops 3537408 | bytes 4730880 | tf_op jit(solution)/shard_map/while/body/eval_jaxpr/reduce_sum | solution.py:82
  194.1 3.0 %bitcast_reduce_fusion.3 = (f32[4,384]{1,0:T(4,128)S(1)}, f32[768,384,4]{1,0,2:T(8,128)}) fusion(bf16[384,4,64]{0,2,1:T(8,128)(2,1)S(1)} %get-tuple-element.203, bf16[768,128]{0,1:T(8,128)(2,1)S(1)} %bitcast.136), kind=kOutput, calls=%fused_computation.4.clone.1 | convolution fusion | flops 153352704 | bytes 5019648 | tf_op jit(solution)/shard_map/while/body/eval_jaxpr/qhd,kd->hqk/dot_general | solution.py:71
  197.1 3.3 %fusion.75 = f32[4,384]{1,0:T(4,128)S(1)} fusion(f32[768,384,4]{1,0,2:T(8,128)} %get-tuple-element.179, f32[4,384]{1,0:T(4,128)S(1)} %select_maximum_fusion.2), kind=kLoop, calls=%fused_computation.7.clone.1 | loop fusion | flops 3537408 | bytes 4730880 | tf_op jit(solution)/shard_map/while/body/eval_jaxpr/reduce_sum | solution.py:82
  203.7 18.2 %reduce-scatter.8.cloned.1.call-done = bf16[384,2048]{1,0:T(8,128)(2,1)} async-done(((bf16[1536,2048]{1,0:T(8,128)(2,1)}), bf16[384,2048]{1,0:T(8,128)(2,1)}) %reduce-scatter.8.cloned.1.call-update) | async-done | bytes 1572880 | tf_op jit(solution)/shard_map/reduce_scatter | solution.py:194
  221.9 4.6 %all-to-all-start.1 = ((bf16[4,96,2048]{2,1,0:T(8,128)(2,1)}), bf16[4,96,2048]{2,1,0:T(8,128)(2,1)S(1)}, u32[]{:S(2)}, u32[]{:S(2)}) async-start(bf16[4,96,2048]{2,1,0:T(8,128)(2,1)} %bitcast.142), calls=%async_computation.4 | async-start | bytes 3145728 | tf_op jit(solution)/shard_map/all_to_all | solution.py:201
  226.8 36.5 %all-to-all-done.1 = bf16[4,96,2048]{2,1,0:T(8,128)(2,1)S(1)} async-done(((bf16[4,96,2048]{2,1,0:T(8,128)(2,1)}), bf16[4,96,2048]{2,1,0:T(8,128)(2,1)S(1)}, u32[]{:S(2)}, u32[]{:S(2)}) %all-to-all-start.1) | async-done | bytes 1572896 | tf_op jit(solution)/shard_map/all_to_all | solution.py:201
  264.5 3.4 %gather_fusion.2 = bf16[128,2048]{1,0:T(8,128)(2,1)S(1)} fusion(bf16[384,2048]{1,0:T(8,128)(2,1)} %bitcast.134, s32[1024]{0:T(1024)S(1)} %get-tuple-element.135), kind=kCustom, calls=%fused_computation.1.clone | custom fusion | bytes 1049088 | tf_op jit(solution)/shard_map/jit(_take)/gather | solution.py:206
  270.2 16.3 %reduce-scatter.4.cloned.1.call-done = bf16[96,2048]{1,0:T(8,128)(2,1)} async-done(((bf16[384,2048]{1,0:T(8,128)(2,1)}), bf16[96,2048]{1,0:T(8,128)(2,1)}) %reduce-scatter.4.cloned.1.call-update) | async-done | bytes 393232 | tf_op jit(solution)/shard_map/reduce_scatter | solution.py:191
  (115 shorter events, 22.4 us)
Async XLA Ops:
  7.2 135.0 %copy-start = (bf16[2,256,2048]{2,1,0:T(8,128)(2,1)S(1)}, bf16[2,256,2048]{2,1,0:T(8,128)(2,1)}, u32[]{:S(2)}) copy-start(bf16[2,256,2048]{2,1,0:T(8,128)(2,1)} %param.30) | copy-start | bytes 6291460
  7.2 128.6 %all-gather.5.cloned.1.call-start = ((), (), s32[]{:S(2)}) async-start(), calls=%async_computation.8 | async-start | bytes 7864320 | tf_op jit(solution)/shard_map/all_gather | solution.py:183
  12.2 3.1 %copy-start.3 = (bf16[128,2048]{1,0:T(8,128)(2,1)}, bf16[128,2048]{1,0:T(8,128)(2,1)S(1)}, u32[]{:S(2)}) copy-start(bf16[128,2048]{1,0:T(8,128)(2,1)S(1)} %fusion.27) | copy-start | bytes 1572868
  90.1 72.6 %all-gather.3.cloned.1.call-start = ((), (), s32[]{:S(2)}) async-start(), calls=%async_computation.6 | async-start | bytes 2621440 | tf_op jit(solution)/shard_map/all_gather | solution.py:175
  90.8 131.1 %reduce-scatter.8.cloned.1.call-start = ((), (), s32[]{:S(2)}) async-start(), calls=%async_computation.9 | async-start | bytes 7864320 | tf_op jit(solution)/shard_map/reduce_scatter | solution.py:194
  159.4 0.9 copy-start.9
  159.5 1.3 copy-start.13
  159.5 1.4 copy-start.8
  159.5 1.7 copy-start.12
  159.5 108.4 %reduce-scatter.6.cloned.1.call-start = ((), (), s32[]{:S(2)}) async-start(), calls=%async_computation.7 | async-start | bytes 2621440 | tf_op jit(solution)/shard_map/reduce_scatter | solution.py:197
  160.5 2.2 copy-start.7
  162.7 2.5 copy-start.5
  170.1 116.4 %reduce-scatter.4.cloned.1.call-start = ((), (), s32[]{:S(2)}) async-start(), calls=%async_computation.5 | async-start | bytes 1966080 | tf_op jit(solution)/shard_map/reduce_scatter | solution.py:191
  185.9 16.0 %copy-start.6 = (bf16[256,2048]{1,0:T(8,128)(2,1)S(1)}, bf16[256,2048]{1,0:T(8,128)(2,1)}, u32[]{:S(2)}) copy-start(bf16[256,2048]{1,0:T(8,128)(2,1)} %param.23) | copy-start | bytes 3145732
  189.1 3.8 %copy-start.2 = (f32[768,384,4]{1,0,2:T(8,128)S(1)}, f32[768,384,4]{1,0,2:T(8,128)}, u32[]{:S(2)}) copy-start(f32[768,384,4]{1,0,2:T(8,128)} %get-tuple-element.179) | copy-start | bytes 14155780 | tf_op jit(solution)/shard_map/while
  197.1 3.8 %copy-start.2 = (f32[768,384,4]{1,0,2:T(8,128)S(1)}, f32[768,384,4]{1,0,2:T(8,128)}, u32[]{:S(2)}) copy-start(f32[768,384,4]{1,0,2:T(8,128)} %get-tuple-element.179) | copy-start | bytes 14155780 | tf_op jit(solution)/shard_map/while
  203.7 23.0 %copy-start.10 = (s32[128,2]{0,1:T(2,128)S(1)}, s32[128,2]{0,1:T(2,128)}, u32[]{:S(2)}) copy-start(s32[128,2]{0,1:T(2,128)} %param.26) | copy-start | bytes 3076
  203.7 23.1 %copy-start.11 = (f32[128,2]{0,1:T(2,128)S(1)}, f32[128,2]{0,1:T(2,128)}, u32[]{:S(2)}) copy-start(f32[128,2]{0,1:T(2,128)} %param.27) | copy-start | bytes 3076
  221.9 41.4 %all-to-all-start.1 = ((bf16[4,96,2048]{2,1,0:T(8,128)(2,1)}), bf16[4,96,2048]{2,1,0:T(8,128)(2,1)S(1)}, u32[]{:S(2)}, u32[]{:S(2)}) async-start(bf16[4,96,2048]{2,1,0:T(8,128)(2,1)} %bitcast.142), calls=%async_computation.4 | async-start | bytes 3145728 | tf_op jit(solution)/shard_map/all_to_all | solution.py:201
  263.3 1.2 copy-start.4
  264.5 22.0 %copy-start.1 = (bf16[2,256,2048]{2,1,0:T(8,128)(2,1)S(1)}, bf16[2,256,2048]{2,1,0:T(8,128)(2,1)}, u32[]{:S(2)}) copy-start(bf16[2,256,2048]{2,1,0:T(8,128)(2,1)} %param.30) | copy-start | bytes 6291460
Sparse Core Ops, SparseCore 0:
  90.2 45.4 all-gather.4
  137.9 22.5 all-gather.2
  163.0 58.8 reduce-scatter.7
  224.3 31.1 reduce-scatter.5
  258.4 28.0 reduce-scatter.3
where the time goes:
time: 294 us; the launch traced here: 293 us
  waiting for transfers between devices  117 us (40%)
  blocking collectives  58 us (20%)
  local copies, waits for them, and re-layouts  36.6 us (12%)
  matrix products  34.1 us (12%)
  other arithmetic  28.3 us (10%)
  between operations  14.2 us (5%)
  starting transfers between devices  5.02 us (2%)
    all_gather x1, waiting for transfers between devices, body(): lax.all_gather(arrived, 'tp', axis=0, tiled=True)  44.9 us
    all_to_all x1, blocking collectives, body(): lax.all_to_all(outgoing, 'ep', split_axis=1, concat_axis=1, tiled=True)  43.4 us
    all_to_all x1, waiting for transfers between devices, body(): lax.all_to_all(routed_sum.astype(jnp.bfloat16), 'ep', split_axis=0, conca...  36.5 us
    reduce_scatter x1, waiting for transfers between devices, body(): lax.psum_scatter(routed_part.astype(jnp.bfloat16), 'tp', scatter_dimensio...  18.2 us
    reduce_scatter x1, waiting for transfers between devices, body(): lax.psum_scatter(head_partial.astype(jnp.bfloat16), 'tp', scatter_dimensi...  16.3 us
    all_gather x1, blocking collectives, body(): lax.all_gather(keys_and_values, 'ep', axis=0, tiled=True)  14.6 us
    unnamed x34, local copies, waits for them, and re-layouts  14.3 us
    unnamed x4, other arithmetic  12.4 us
  transfers between devices with their start and end apart: 6, of which 4 were waited for; matrix products, arithmetic and copies ran while one was open for 20% of the time, Pallas kernels for 0%

commit v1 on v0

v1 whole, which is shorter than its diff:
```python
import functools

import jax
import jax.numpy as jnp
from jax import lax
from jax.experimental import pallas as pl
from jax.experimental.pallas import tpu as pltpu
from jax.sharding import PartitionSpec as P

GRID_W = 64


rope_base = 10000.0
norm_eps = 1e-06


def head_norm(vectors, gain):
    return (
        vectors * lax.rsqrt(jnp.mean(vectors * vectors, axis=-1, keepdims=True) + norm_eps) * gain
    )


def turn_heads(vectors, positions):
    row_count, head_count, head_size = vectors.shape
    half_size = head_size // 2
    inverse = rope_base ** (-jnp.arange(0, half_size, 2, dtype=jnp.float32) / half_size)
    grid_row = (positions // GRID_W).astype(jnp.float32)
    grid_column = (positions % GRID_W).astype(jnp.float32)
    angles = jnp.concatenate([grid_row[:, None] * inverse, grid_column[:, None] * inverse], axis=-1)
    cosine = jnp.cos(angles)[:, None, :]
    sine = jnp.sin(angles)[:, None, :]
    paired = vectors.reshape(row_count, head_count, half_size, 2)
    first = paired[..., 0]
    second = paired[..., 1]
    turned = jnp.stack([first * cosine - second * sine, first * sine + second * cosine], axis=-1)
    return turned.reshape(vectors.shape)


def slot_ids(route_rows, expert_count, capacity):
    row_count, top_count = route_rows.shape
    flat_routes = route_rows.reshape(-1)
    pair_count = row_count * top_count
    onehot = flat_routes[:, None] == jnp.arange(expert_count, dtype=jnp.int32)[None, :]
    order = jnp.arange(pair_count, dtype=jnp.int32)
    before = (order[None, :] < order[:, None]).astype(jnp.bfloat16)
    earlier = jnp.dot(before, onehot.astype(jnp.bfloat16), preferred_element_type=jnp.float32)
    within = jnp.sum(jnp.where(onehot, earlier, 0.0), axis=1).astype(jnp.int32)
    return (flat_routes * capacity + within).reshape(row_count, top_count)


MESH = pl.DeviceIdType.MESH


def greet(ep_count, tp_count, e, t):
    barrier = pltpu.get_barrier_semaphore()
    peers = 0
    for d in range(1, ep_count):
        pl.semaphore_signal(
            barrier, inc=1, device_id={"ep": lax.rem(e + d, ep_count)}, device_id_type=MESH
        )
        peers += 1
    pair = t // 2
    core = lax.rem(t, 2)
    for k in range(1, tp_count // 2):
        pl.semaphore_signal(
            barrier,
            inc=1,
            device_id={"tp": lax.rem(pair + k, tp_count // 2) * 2 + core},
            device_id_type=MESH,
        )
        peers += 1
    pl.semaphore_signal(
        barrier, inc=1, device_id={"tp": pair * 2 + 1 - core}, device_id_type=MESH
    )
    peers += 1
    pl.semaphore_wait(barrier, peers)


def remote(src, dst, send, recv, device):
    return pltpu.make_async_remote_copy(
        src_ref=src,
        dst_ref=dst,
        send_sem=send,
        recv_sem=recv,
        device_id=device,
        device_id_type=MESH,
    )


def dispatch_kernel(
    ep_count,
    tp_count,
    blocks,
    normed,
    kv,
    arrived,
    normed_all,
    kv_all,
    local_sem,
    kv_send,
    kv_recv,
    z_send,
    z_recv,
    x_send,
    x_recv,
    d_send,
    d_recv,
):
    e = lax.axis_index("ep")
    t = lax.axis_index("tp")
    half = tp_count // 2
    pair = t // 2
    core = lax.rem(t, 2)
    sibling = {"tp": pair * 2 + 1 - core}
    greet(ep_count, tp_count, e, t)

    sends = []
    for d in range(1, ep_count):
        there = lax.rem(e + d, ep_count)
        copy = remote(kv, kv_all.at[e], kv_send.at[d], kv_recv.at[e], {"ep": there})
        copy.start()
        sends.append(copy)
    for d in range(1, ep_count):
        there = lax.rem(e + d, ep_count)
        copy = remote(
            blocks.at[there], arrived.at[:, t, e], z_send.at[d], z_recv.at[e], {"ep": there}
        )
        copy.start()
        sends.append(copy)

    def place(item, row):
        if item is None:
            return normed_all.at[row]
        return arrived.at[:, row, item]

    def spread(src, item, number):
        for k in range(1, half):
            other = lax.rem(pair + k, half)
            copy = remote(
                src,
                place(item, t),
                x_send.at[k, number],
                x_recv.at[pair, number],
                {"tp": other * 2 + core},
            )
            copy.start()
            sends.append(copy)
        copy = remote(
            src, place(item, t), d_send.at[0, number], d_recv.at[pair, number], sibling
        )
        copy.start()
        sends.append(copy)

    def pass_on(item, number):
        for k in range(1, half):
            other = lax.rem(pair + k, half)
            row = other * 2 + core
            spot = place(item, row)
            remote(spot, spot, x_send.at[k, number], x_recv.at[other, number], sibling).wait_recv()
            copy = remote(spot, spot, d_send.at[k, number], d_recv.at[other, number], sibling)
            copy.start()
            sends.append(copy)

    spread(blocks.at[e], e, 0)
    spread(normed, None, ep_count)
    own = [
        pltpu.make_async_copy(blocks.at[e], arrived.at[:, t, e], local_sem.at[0]),
        pltpu.make_async_copy(normed, normed_all.at[t], local_sem.at[1]),
        pltpu.make_async_copy(kv, kv_all.at[e], local_sem.at[2]),
    ]
    for copy in own:
        copy.start()

    pass_on(e, 0)
    pass_on(None, ep_count)
    for d in range(1, ep_count):
        source = lax.rem(e - d + ep_count, ep_count)
        spot = arrived.at[:, t, source]
        remote(spot, spot, z_send.at[d], z_recv.at[source], sibling).wait_recv()
        spread(spot, source, d)
        if d > 1:
            pass_on(lax.rem(e - d + 1 + ep_count, ep_count), d - 1)
    if ep_count > 1:
        pass_on(lax.rem(e + 1, ep_count), ep_count - 1)

    for d in range(1, ep_count):
        source = lax.rem(e - d + ep_count, ep_count)
        spot = kv_all.at[source]
        remote(spot, spot, kv_send.at[d], kv_recv.at[source], sibling).wait_recv()
    for number in range(ep_count + 1):
        item = None if number == ep_count else lax.rem(e - number + ep_count, ep_count)
        for other in range(half):
            spot = place(item, other * 2 + 1 - core)
            remote(spot, spot, d_send.at[0, number], d_recv.at[other, number], sibling).wait_recv()
    for copy in own:
        copy.wait()
    for copy in sends:
        copy.wait_send()


def dispatch(ep_count, tp_count, blocks, normed, kv):
    locals_here, capacity, width = blocks.shape[1:]
    vmem = pl.BlockSpec(memory_space=pltpu.VMEM)
    half = tp_count // 2
    dma = pltpu.SemaphoreType.DMA
    return pl.pallas_call(
        functools.partial(dispatch_kernel, ep_count, tp_count),
        out_shape=(
            jax.ShapeDtypeStruct(
                (locals_here, tp_count, ep_count, capacity, width), jnp.bfloat16
            ),
            jax.ShapeDtypeStruct((tp_count,) + normed.shape, jnp.bfloat16),
            jax.ShapeDtypeStruct((ep_count,) + kv.shape, jnp.bfloat16),
        ),
        in_specs=[vmem] * 3,
        out_specs=(vmem,) * 3,
        scratch_shapes=[
            dma((3,)),
            dma((ep_count,)),
            dma((ep_count,)),
            dma((ep_count,)),
            dma((ep_count,)),
            dma((half, ep_count + 1)),
            dma((half, ep_count + 1)),
            dma((half, ep_count + 1)),
            dma((half, ep_count + 1)),
        ],
        compiler_params=pltpu.CompilerParams(collective_id=0, has_side_effects=True),
    )(blocks, normed, kv)


def collect_kernel(
    ep_count,
    tp_count,
    routed,
    shared,
    mixed,
    returned,
    shared_sum,
    mixed_sum,
    routed_pair,
    routed_out,
    routed_in,
    routed_done,
    shared_pair,
    shared_out,
    shared_in,
    mixed_pair,
    mixed_out,
    mixed_in,
    d_send,
    d_recv,
    x_send,
    x_recv,
    z_send,
    z_recv,
):
    e = lax.axis_index("ep")
    t = lax.axis_index("tp")
    half = tp_count // 2
    pair = t // 2
    core = lax.rem(t, 2)
    sibling = {"tp": pair * 2 + 1 - core}
    greet(ep_count, tp_count, e, t)

    def item(number):
        if number < ep_count:
            place = lax.rem(e + number + 1, ep_count)
            return (
                lambda row: routed.at[:, row, place],
                lambda k: routed_pair.at[number, k],
                lambda k: routed_out.at[number, k],
                lambda k: routed_in.at[number, k],
            )
        if number == ep_count:
            return (
                lambda row: shared.at[row],
                lambda k: shared_pair.at[k],
                lambda k: shared_out.at[k],
                lambda k: shared_in.at[k],
            )
        return (
            lambda row: mixed.at[row],
            lambda k: mixed_pair.at[k],
            lambda k: mixed_out.at[k],
            lambda k: mixed_in.at[k],
        )

    count = ep_count + 2
    sends = []
    for number in range(count):
        part, paired, out, into = item(number)
        for k in list(range(1, half)) + [0]:
            other = lax.rem(pair + k, half)
            copy = remote(
                part(other * 2 + 1 - core),
                paired(k),
                d_send.at[number, k],
                d_recv.at[number, k],
                sibling,
            )
            copy.start()
            sends.append(copy)

    def both(number, k):
        part, paired, out, into = item(number)
        spot = paired(k)
        remote(spot, spot, d_send.at[number, k], d_recv.at[number, k], sibling).wait_recv()
        mine = part(lax.rem(pair + k, half) * 2 + core)
        return mine[...].astype(jnp.float32) + spot[...].astype(jnp.float32)

    for number in range(count):
        part, paired, out, into = item(number)
        for k in range(1, half):
            other = lax.rem(pair + k, half)
            out(k)[...] = both(number, k).astype(jnp.bfloat16)
            copy = remote(
                out(k),
                into(k),
                x_send.at[number, k],
                x_recv.at[number, k],
                {"tp": other * 2 + core},
            )
            copy.start()
            sends.append(copy)
    for number in range(count):
        part, paired, out, into = item(number)
        total = both(number, 0)
        for k in range(1, half):
            spot = into(k)
            remote(spot, spot, x_send.at[number, k], x_recv.at[number, k], sibling).wait_recv()
            total = total + spot[...].astype(jnp.float32)
        if number < ep_count - 1:
            place = lax.rem(e + number + 1, ep_count)
            routed_done[number] = total.astype(jnp.bfloat16)
            copy = remote(
                routed_done.at[number],
                returned.at[e],
                z_send.at[number],
                z_recv.at[e],
                {"ep": place},
            )
            copy.start()
            sends.append(copy)
        elif number == ep_count - 1:
            returned[e] = total.astype(jnp.bfloat16)
        elif number == ep_count:
            shared_sum[...] = total
        else:
            mixed_sum[...] = total.astype(jnp.bfloat16)
    for d in range(1, ep_count):
        source = lax.rem(e - d + ep_count, ep_count)
        spot = returned.at[source]
        remote(spot, spot, z_send.at[0], z_recv.at[source], sibling).wait_recv()
    for copy in sends:
        copy.wait_send()


def collect(ep_count, tp_count, routed, shared, mixed):
    locals_here, capacity, width = routed.shape[0], routed.shape[3], routed.shape[4]
    vmem = pl.BlockSpec(memory_space=pltpu.VMEM)
    half = tp_count // 2
    dma = pltpu.SemaphoreType.DMA
    block = (locals_here, capacity, width)
    count = ep_count + 2
    return pl.pallas_call(
        functools.partial(collect_kernel, ep_count, tp_count),
        out_shape=(
            jax.ShapeDtypeStruct((ep_count,) + block, jnp.bfloat16),
            jax.ShapeDtypeStruct(shared.shape[1:], jnp.float32),
            jax.ShapeDtypeStruct(mixed.shape[1:], jnp.bfloat16),
        ),
        in_specs=[vmem] * 3,
        out_specs=(vmem,) * 3,
        scratch_shapes=[
            pltpu.VMEM((ep_count, half) + block, jnp.bfloat16),
            pltpu.VMEM((ep_count, half) + block, jnp.bfloat16),
            pltpu.VMEM((ep_count, half) + block, jnp.bfloat16),
            pltpu.VMEM((ep_count,) + block, jnp.bfloat16),
            pltpu.VMEM((half,) + shared.shape[1:], jnp.bfloat16),
            pltpu.VMEM((half,) + shared.shape[1:], jnp.bfloat16),
            pltpu.VMEM((half,) + shared.shape[1:], jnp.bfloat16),
            pltpu.VMEM((half,) + mixed.shape[1:], jnp.bfloat16),
            pltpu.VMEM((half,) + mixed.shape[1:], jnp.bfloat16),
            pltpu.VMEM((half,) + mixed.shape[1:], jnp.bfloat16),
            dma((count, half)),
            dma((count, half)),
            dma((count, half)),
            dma((count, half)),
            dma((ep_count,)),
            dma((ep_count,)),
        ],
        compiler_params=pltpu.CompilerParams(
            collective_id=1, has_side_effects=True, vmem_limit_bytes=67043328
        ),
    )(routed, shared, mixed)


def pick_block(row_count):
    for candidate in range(min(row_count, 1024), 0, -1):
        if row_count % candidate == 0:
            return candidate
    return row_count


def attend_keys(query_turned, scale, running, pieces):
    head_size = query_turned.shape[-1]
    key_block = pick_block(pieces.shape[0])
    blocks = pieces.reshape(pieces.shape[0] // key_block, key_block, 2 * head_size)

    def one_block(carried, block_rows):
        top_now, total_now, acc_now = carried
        scores = (
            jnp.einsum(
                "qhd,kd->hqk",
                query_turned,
                block_rows[:, :head_size],
                preferred_element_type=jnp.float32,
            )
            * scale
        )
        top_new = jnp.maximum(top_now, jnp.max(scores, axis=-1))
        shrink = jnp.exp(top_now - top_new)
        exps = jnp.exp(scores - top_new[..., None])
        total_new = total_now * shrink + jnp.sum(exps, axis=-1)
        acc_new = acc_now * shrink[..., None] + jnp.einsum(
            "hqk,kd->hqd",
            exps.astype(jnp.bfloat16),
            block_rows[:, head_size:],
            preferred_element_type=jnp.float32,
        )
        return ((top_new, total_new, acc_new), None)

    result, ignored = lax.scan(one_block, running, blocks)
    return result


def shared_hidden_of(token_rows, gate_weights, up_weights):
    gate_part = jnp.dot(token_rows, gate_weights, preferred_element_type=jnp.float32)
    up_part = jnp.dot(token_rows, up_weights, preferred_element_type=jnp.float32)
    return (jax.nn.silu(gate_part) * up_part).astype(jnp.bfloat16)


def body(
    queries,
    key_values,
    query_gain,
    key_gain,
    out_weight,
    second_batch,
    norm_gain,
    routes,
    route_weights,
    expert_gate,
    expert_up,
    expert_down,
    shared_gate,
    shared_up,
    shared_down,
):
    query_rows = queries.shape[0]
    head_size = query_gain.shape[0]
    heads_here = queries.shape[1] // head_size
    ep_count = lax.axis_size("ep")
    tp_count = lax.axis_size("tp")
    positions = lax.axis_index("ep") * query_rows + jnp.arange(query_rows, dtype=jnp.int32)
    query_turned = turn_heads(
        head_norm(
            queries.reshape(query_rows, heads_here, head_size).astype(jnp.float32), query_gain
        ),
        positions,
    ).astype(jnp.bfloat16)
    key_turned = turn_heads(
        head_norm(key_values[:, None, :head_size].astype(jnp.float32), key_gain), positions
    ).astype(jnp.bfloat16)
    keys_and_values = jnp.concatenate([key_turned[:, 0, :], key_values[:, head_size:]], axis=1)
    tok_count = second_batch.shape[0]
    model_width = second_batch.shape[1]
    top_count = routes.shape[1]
    local_experts = expert_gate.shape[0]
    expert_count = local_experts * ep_count
    capacity = 3 * tok_count * top_count // (2 * expert_count)
    slot_count = expert_count * capacity
    token_float = second_batch.astype(jnp.float32)
    normed = (
        token_float
        * lax.rsqrt(jnp.mean(token_float * token_float, axis=-1, keepdims=True) + norm_eps)
        * norm_gain
    ).astype(jnp.bfloat16)
    own_slots = slot_ids(routes, expert_count, capacity)
    slot_numbers = jnp.arange(slot_count, dtype=jnp.int32)
    picks = [
        (own_slots[:, j][:, None] == slot_numbers[None, :]).astype(jnp.bfloat16)
        for j in range(top_count)
    ]
    outgoing = lax.dot_general(
        sum(picks), normed, (((0,), (0,)), ((), ())), preferred_element_type=jnp.float32
    ).astype(jnp.bfloat16)
    arrived, normed_all, kv_all = dispatch(
        ep_count,
        tp_count,
        outgoing.reshape(ep_count, local_experts, capacity, model_width),
        normed,
        keys_and_values,
    )
    start_state = (
        jnp.full((heads_here, query_rows), -1e30, jnp.float32),
        jnp.zeros((heads_here, query_rows), jnp.float32),
        jnp.zeros((heads_here, query_rows, head_size), jnp.float32),
    )
    top_all, total_all, acc_all = attend_keys(
        query_turned,
        head_size ** (-0.5),
        start_state,
        kv_all.reshape(ep_count * query_rows, 2 * head_size),
    )
    head_out = (
        (acc_all / total_all[..., None])
        .transpose(1, 0, 2)
        .reshape(query_rows, heads_here * head_size)
        .astype(jnp.bfloat16)
    )
    head_partial = jnp.dot(head_out, out_weight, preferred_element_type=jnp.float32)
    shared_hidden = shared_hidden_of(
        normed_all.reshape(tp_count * tok_count, model_width), shared_gate, shared_up
    )
    shared_part = jnp.dot(shared_hidden, shared_down, preferred_element_type=jnp.float32)
    slot_rows = arrived.reshape(local_experts, tp_count * ep_count * capacity, model_width)
    gate_part = jnp.einsum(
        "jmd,jdf->jmf", slot_rows, expert_gate, preferred_element_type=jnp.float32
    )
    up_part = jnp.einsum("jmd,jdf->jmf", slot_rows, expert_up, preferred_element_type=jnp.float32)
    hidden = (jax.nn.silu(gate_part) * up_part).astype(jnp.bfloat16)
    routed_part = jnp.einsum(
        "jmf,jfd->jmd", hidden, expert_down, preferred_element_type=jnp.float32
    )
    returned, shared_sum, mixer_out = collect(
        ep_count,
        tp_count,
        routed_part.astype(jnp.bfloat16).reshape(arrived.shape),
        shared_part.astype(jnp.bfloat16).reshape(normed_all.shape),
        head_partial.astype(jnp.bfloat16).reshape(tp_count, query_rows // tp_count, model_width),
    )
    returned = returned.reshape(slot_count, model_width)
    combined = shared_sum
    for j in range(top_count):
        combined = combined + route_weights[:, j : j + 1] * jnp.dot(
            picks[j], returned, preferred_element_type=jnp.float32
        )
    return (mixer_out, combined.astype(jnp.bfloat16))


def solution(mesh):
    placed = (
        P(("grp", "ep"), "tp"),
        P(("grp", "ep"), "tp"),
        P(),
        P(),
        P("tp", None),
        P(("grp", "ep", "tp"), None),
        P(),
        P(("grp", "ep", "tp"), None),
        P(("grp", "ep", "tp"), None),
        P("ep", None, "tp"),
        P("ep", None, "tp"),
        P("ep", "tp", None),
        P(None, "tp"),
        P(None, "tp"),
        P("tp", None),
    )
    return jax.shard_map(
        body,
        mesh=mesh,
        in_specs=placed,
        out_specs=(P(("grp", "ep", "tp"), None), P(("grp", "ep", "tp"), None)),
        check_vma=False,
    )
```

time: 294 us -> 195 us (0.66)
  Pallas kernels: 0 us -> 138 us
  waiting for transfers between devices: 117 us -> 0 us
  blocking collectives: 58 us -> 0 us
  local copies, waits for them, and re-layouts: 36.6 us -> 5.06 us
  other arithmetic: 28.3 us -> 12.4 us
  between operations: 14.2 us -> 1 us
  starting transfers between devices: 5.02 us -> 0 us
  matrix products: 34.1 us -> 37.7 us
    pallas_call x0 -> x2, Pallas kernels: none -> 138 us  [the longest x1 72.7 us: collect(): pl.pallas_call(functools.partial(collect_kernel, ep_count, tp_count), out...]
    all_gather x2 -> x0, waiting for transfers between devices: 44.9 us -> none  [the longest x1 44.9 us: body(): lax.all_gather(arrived, 'tp', axis=0, tiled=True)]
    all_to_all x1 -> x0, blocking collectives: 43.4 us -> none  [body(): lax.all_to_all(outgoing, 'ep', split_axis=1, concat_axis=1, tiled=True)]
    all_to_all x1 -> x0, waiting for transfers between devices: 36.5 us -> none  [body(): lax.all_to_all(routed_sum.astype(jnp.bfloat16), 'ep', split_axis=0, conca...]
    reduce_scatter x3 -> x0, waiting for transfers between devices: 34.5 us -> none  [the longest x1 18.2 us: body(): lax.psum_scatter(routed_part.astype(jnp.bfloat16), 'tp', scatter_dimensio...]
    all_gather x1 -> x0, blocking collectives: 14.6 us -> none  [body(): lax.all_gather(keys_and_values, 'ep', axis=0, tiled=True)]
    unnamed x34 -> x32, local copies, waits for them, and re-layouts: 14.3 us -> 1.88 us
    unnamed x4 -> x3, other arithmetic: 12.4 us -> 0.01 us
  transfers between devices with their start and end apart: 6 -> 0, of which waited for: 4 -> 0; matrix products, arithmetic and copies ran while one was open for 20% -> 0% of each run, Pallas kernels for 0% -> 0%
where the time goes in v1:
time: 195 us
  Pallas kernels  138 us (71%)
  matrix products  37.7 us (19%)
  other arithmetic  12.4 us (6%)
  local copies, waits for them, and re-layouts  5.06 us (3%)
    pallas_call x1, Pallas kernels, collect(): pl.pallas_call(functools.partial(collect_kernel, ep_count, tp_count), out...  72.7 us
    pallas_call x1, Pallas kernels, dispatch(): pl.pallas_call(functools.partial(dispatch_kernel, ep_count, tp_count), ou...  65.4 us
    dot_general x1, matrix products, body(): jnp.einsum('jmf,jfd->jmd', hidden, expert_down, preferred_element_type=jn...  10.9 us
    reduce_sum x2, other arithmetic, one_block(): total_new = total_now * shrink + jnp.sum(exps, axis=-1)  6.54 us
    dot_general x2, matrix products, one_block(): jnp.einsum('qhd,kd->hqk', query_turned, block_rows[:, :head_size], prefer...  6.05 us
    dot_general x1, matrix products, body(): jnp.einsum('jmd,jdf->jmf', slot_rows, expert_gate, preferred_element_type...  5.77 us
    dot_general x1, matrix products, body(): jnp.dot(shared_hidden, shared_down, preferred_element_type=jnp.float32)  4.93 us

profile of v1, /device:TPU:0, one launch (start us, length us, event | category | flops | bytes accessed | tf_op | source)
XLA Modules:
  0.0 194.5 jit_solution(12565592073209038292)
XLA Ops:
  0.6 1.3 fusion.16
  1.9 1.2 fusion.18.normed
  3.2 0.8 copy.42
  4.5 0.7 multiply_add_fusion
  5.3 1.8 convolution_convert_fusion.3
  8.2 0.7 pad_maximum_fusion.1.kv
  8.9 65.4 %shard_map.158 = (bf16[2,4,4,48,2048]{4,3,2,1,0:T(8,128)(2,1)}, bf16[4,128,2048]{2,1,0:T(8,128)(2,1)}, bf16[4,384,128]{2,1,0:T(8,128)(2,1)S(1)}) custom-call(bf16[4,2,48,2048]{3,2,1,0:T(8,128)(2,1)} %bitcast.93, bf16[128,2048]{1,0:T(8,128)(2,1)} %copy-done.3, bf16[384,128]{1,0:T(8,128)(2,1)} %pad_maximum_fusion.1.kv), custom_call_target="tpu_custom_call" | custom-call | tf_op jit(solution)/shard_map/pallas_call | solution.py:206
  74.3 5.8 %fusion.53 = f32[2,768,256]{2,1,0:T(8,128)} fusion(bf16[2,768,2048]{2,1,0:T(8,128)(2,1)} %bitcast.96, bf16[2,2048,256]{2,1,0:T(8,128)(2,1)S(1)} %copy-done.14), kind=kOutput, calls=%fused_computation.105 | convolution fusion | flops 1610612736 | bytes 9961472 | tf_op jit(solution)/shard_map/jmd,jdf->jmf/dot_general | solution.py:529
  80.1 10.9 %convolution_convert_fusion = bf16[2,768,2048]{2,1,0:T(8,128)(2,1)} fusion(bf16[2,256,2048]{2,1,0:T(8,128)(2,1)} %param.28, f32[2,768,256]{2,1,0:T(8,128)} %fusion.53, bf16[2,768,2048]{2,1,0:T(8,128)(2,1)} %bitcast.97, bf16[2,2048,256]{2,1,0:T(8,128)(2,1)} %param.27), kind=kOutput, calls=%fused_computation.17 | convolution fusion | flops 3226730496 | bytes 18350080 | tf_op jit(solution)/shard_map/jmf,jfd->jmd/dot_general | solution.py:534
  90.9 0.7 fusion.54
  91.7 4.9 %convolution_convert_fusion.1 = bf16[512,2048]{1,0:T(8,128)(2,1)} fusion(bf16[128,2048]{1,0:T(8,128)(2,1)} %param.31, bf16[512,2048]{1,0:T(8,128)(2,1)S(1)} %bitcast.88, bf16[2048,128]{1,0:T(8,128)(2,1)} %param.30, f32[512,128]{1,0:T(8,128)S(1)} %fusion.54), kind=kOutput, calls=%fused_computation.18 | convolution fusion | flops 538312704 | bytes 5505024 | tf_op jit(solution)/shard_map/dot_general | solution.py:527
  98.6 16.1 %while.15 = (s32[]{:T(128)}, f32[4,384]{1,0:T(4,128)S(1)}, f32[4,384]{1,0:T(4,128)S(1)}, f32[4,384,64]{1,2,0:T(8,128)S(1)}, bf16[2,768,128]{2,1,0:T(8,128)(2,1)S...) while((s32[]{:T(128)}, f32[4,384]{1,0:T(4,128)S(1)}, f32[4,384]{1,0:T(4,128)S(1)}, ...), condition=%wide.region_7.8_spmd.clone, body=%wide.region_4.7_spmd.clone.sunk | while | flops 311729664 | bytes 35094664 | solution.py:434
  98.8 3.0 %bitcast_reduce_fusion.3 = (f32[4,384]{1,0:T(4,128)S(1)}, f32[768,384,4]{1,0,2:T(8,128)}) fusion(bf16[384,4,64]{0,2,1:T(8,128)(2,1)S(1)} %get-tuple-element.198, bf16[768,128]{0,1:T(8,128)(2,1)S(1)} %bitcast.84), kind=kOutput, calls=%fused_computation.1.clone.1 | convolution fusion | flops 153352704 | bytes 5019648 | tf_op jit(solution)/shard_map/while/body/eval_jaxpr/qhd,kd->hqk/dot_general | solution.py:414
  101.8 3.3 %fusion.78 = f32[4,384]{1,0:T(4,128)S(1)} fusion(f32[768,384,4]{1,0,2:T(8,128)} %get-tuple-element.174, f32[4,384]{1,0:T(4,128)S(1)} %select_maximum_fusion.2), kind=kLoop, calls=%fused_computation.4.clone.1 | loop fusion | flops 3537408 | bytes 4730880 | tf_op jit(solution)/shard_map/while/body/eval_jaxpr/reduce_sum | solution.py:425
  105.6 1.0 fusion.80
  106.8 3.0 %bitcast_reduce_fusion.3 = (f32[4,384]{1,0:T(4,128)S(1)}, f32[768,384,4]{1,0,2:T(8,128)}) fusion(bf16[384,4,64]{0,2,1:T(8,128)(2,1)S(1)} %get-tuple-element.198, bf16[768,128]{0,1:T(8,128)(2,1)S(1)} %bitcast.84), kind=kOutput, calls=%fused_computation.1.clone.1 | convolution fusion | flops 153352704 | bytes 5019648 | tf_op jit(solution)/shard_map/while/body/eval_jaxpr/qhd,kd->hqk/dot_general | solution.py:414
  109.8 3.3 %fusion.78 = f32[4,384]{1,0:T(4,128)S(1)} fusion(f32[768,384,4]{1,0,2:T(8,128)} %get-tuple-element.174, f32[4,384]{1,0:T(4,128)S(1)} %select_maximum_fusion.2), kind=kLoop, calls=%fused_computation.4.clone.1 | loop fusion | flops 3537408 | bytes 4730880 | tf_op jit(solution)/shard_map/while/body/eval_jaxpr/reduce_sum | solution.py:425
  113.6 1.0 fusion.80
  114.8 1.9 convolution_convert_fusion.2
  116.7 72.7 %shard_map.159 = (bf16[4,2,48,2048]{3,2,1,0:T(8,128)(2,1)}, f32[128,2048]{1,0:T(8,128)}, bf16[96,2048]{1,0:T(8,128)(2,1)}) custom-call(bf16[2,4,4,48,2048]{4,3,2,1,0:T(8,128)(2,1)} %bitcast.89, bf16[4,128,2048]{2,1,0:T(8,128)(2,1)} %bitcast.86, bf16[4,96,2048]{2,1,0:T(8,128)(2,1)} %bitcast.92), custom_call_target="tpu_custom_call" | custom-call | tf_op jit(solution)/shard_map/pallas_call | solution.py:366
  189.4 0.8 slice_bitcast_fusion.4
  190.3 2.2 %fusion.12 = f32[128,2048]{1,0:T(8,128)S(1)} fusion(f32[128,2048]{1,0:T(8,128)} %get-tuple-element.47, bf16[384,2048]{1,0:T(8,128)(2,1)} %bitcast.90, f32[128]{0:T(128)S(1)} %get-tuple-element.125, s32[128]{0:T(128)} %copy-done.11), kind=kOutput, calls=%fused_computation.24 | convolution fusion | flops 201900032 | bytes 3671040 | tf_op jit(solution)/shard_map/dot_general | solution.py:547
  192.5 1.3 fusion.13
  193.8 0.7 copy.75
  (78 shorter events, 4.8 us)
Async XLA Ops:
  0.6 6.5 %copy-start.7 = (bf16[384,128]{1,0:T(8,128)(2,1)S(1)}, bf16[384,128]{1,0:T(8,128)(2,1)}, u32[]{:S(2)}) copy-start(bf16[384,128]{1,0:T(8,128)(2,1)} %param.18) | copy-start | bytes 294916
  1.9 5.5 %copy-start.12 = (f32[64]{0:T(128)S(1)}, f32[64]{0:T(128)}, u32[]{:S(2)}) copy-start(f32[64]{0:T(128)} %param.20) | copy-start | bytes 772
  3.2 4.9 %copy-start.3 = (bf16[128,2048]{1,0:T(8,128)(2,1)}, bf16[128,2048]{1,0:T(8,128)(2,1)S(1)}, u32[]{:S(2)}) copy-start(bf16[128,2048]{1,0:T(8,128)(2,1)S(1)} %fusion.18.normed) | copy-start | bytes 1572868
  5.3 2.0 %copy-start.9 = (s32[128]{0:T(128)}, s32[128]{0:T(128)S(1)}, u32[]{:S(2)}) copy-start(s32[128]{0:T(128)S(1)} %get-tuple-element.127) | copy-start | bytes 1540
  5.3 2.0 %copy-start.11 = (s32[128]{0:T(128)}, s32[128]{0:T(128)S(1)}, u32[]{:S(2)}) copy-start(s32[128]{0:T(128)S(1)} %get-tuple-element.126) | copy-start | bytes 1540
  7.2 67.1 %copy-start.14 = (bf16[2,2048,256]{2,1,0:T(8,128)(2,1)S(1)}, bf16[2,2048,256]{2,1,0:T(8,128)(2,1)}, u32[]{:S(2)}) copy-start(bf16[2,2048,256]{2,1,0:T(8,128)(2,1)} %param.26) | copy-start | bytes 6291460
  80.1 10.9 %copy-start.1 = (bf16[4,128,2048]{2,1,0:T(8,128)(2,1)S(1)}, bf16[4,128,2048]{2,1,0:T(8,128)(2,1)}, u32[]{:S(2)}) copy-start(bf16[4,128,2048]{2,1,0:T(8,128)(2,1)} %get-tuple-element.42) | copy-start | bytes 6291460
  80.1 10.9 %copy-start.5 = (bf16[2048,128]{1,0:T(8,128)(2,1)S(1)}, bf16[2048,128]{1,0:T(8,128)(2,1)}, u32[]{:S(2)}) copy-start(bf16[2048,128]{1,0:T(8,128)(2,1)} %param.29) | copy-start | bytes 1572868
  91.6 5.0 %copy-start.8 = (bf16[384,256]{1,0:T(8,128)(2,1)S(1)}, bf16[384,256]{1,0:T(8,128)(2,1)}, u32[]{:S(2)}) copy-start(bf16[384,256]{1,0:T(8,128)(2,1)} %param.17) | copy-start | bytes 589828
  91.7 5.3 %copy-start.13 = (f32[64]{0:T(128)S(1)}, f32[64]{0:T(128)}, u32[]{:S(2)}) copy-start(f32[64]{0:T(128)} %param.19) | copy-start | bytes 772
  98.6 16.2 %copy-start.4 = (bf16[256,2048]{1,0:T(8,128)(2,1)S(1)}, bf16[256,2048]{1,0:T(8,128)(2,1)}, u32[]{:S(2)}) copy-start(bf16[256,2048]{1,0:T(8,128)(2,1)} %param.21) | copy-start | bytes 3145732
  101.8 3.8 %copy-start = (f32[768,384,4]{1,0,2:T(8,128)S(1)}, f32[768,384,4]{1,0,2:T(8,128)}, u32[]{:S(2)}) copy-start(f32[768,384,4]{1,0,2:T(8,128)} %get-tuple-element.174) | copy-start | bytes 14155780 | tf_op jit(solution)/shard_map/while
  109.8 3.8 %copy-start = (f32[768,384,4]{1,0,2:T(8,128)S(1)}, f32[768,384,4]{1,0,2:T(8,128)}, u32[]{:S(2)}) copy-start(f32[768,384,4]{1,0,2:T(8,128)} %get-tuple-element.174) | copy-start | bytes 14155780 | tf_op jit(solution)/shard_map/while
  189.4 3.0 %copy-start.2 = (bf16[4,2,48,2048]{3,2,1,0:T(8,128)(2,1)S(1)}, bf16[4,2,48,2048]{3,2,1,0:T(8,128)(2,1)}, u32[]{:S(2)}) copy-start(bf16[4,2,48,2048]{3,2,1,0:T(8,128)(2,1)} %get-tuple-element.48) | copy-start | bytes 4718596
  189.4 3.0 %copy-start.10 = (s32[128]{0:T(128)S(1)}, s32[128]{0:T(128)}, u32[]{:S(2)}) copy-start(s32[128]{0:T(128)} %copy-done.9) | copy-start | bytes 1540
  192.4 1.3 copy-start.6

commit v2 on v0

v2 whole, which is shorter than its diff:
```python
import functools

import jax
import jax.numpy as jnp
from jax import lax
from jax.experimental import pallas as pl
from jax.experimental.pallas import tpu as pltpu
from jax.sharding import PartitionSpec as P

GRID_W = 64


rope_base = 10000.0
norm_eps = 1e-06


def head_norm(vectors, gain):
    return (
        vectors * lax.rsqrt(jnp.mean(vectors * vectors, axis=-1, keepdims=True) + norm_eps) * gain
    )


def turn_heads(vectors, positions):
    row_count, head_count, head_size = vectors.shape
    half_size = head_size // 2
    inverse = rope_base ** (-jnp.arange(0, half_size, 2, dtype=jnp.float32) / half_size)
    grid_row = (positions // GRID_W).astype(jnp.float32)
    grid_column = (positions % GRID_W).astype(jnp.float32)
    angles = jnp.concatenate([grid_row[:, None] * inverse, grid_column[:, None] * inverse], axis=-1)
    cosine = jnp.cos(angles)[:, None, :]
    sine = jnp.sin(angles)[:, None, :]
    paired = vectors.reshape(row_count, head_count, half_size, 2)
    first = paired[..., 0]
    second = paired[..., 1]
    turned = jnp.stack([first * cosine - second * sine, first * sine + second * cosine], axis=-1)
    return turned.reshape(vectors.shape)


def slot_ids(route_rows, expert_count, capacity):
    row_count, top_count = route_rows.shape
    flat_routes = route_rows.reshape(-1)
    pair_count = row_count * top_count
    onehot = flat_routes[:, None] == jnp.arange(expert_count, dtype=jnp.int32)[None, :]
    order = jnp.arange(pair_count, dtype=jnp.int32)
    before = (order[None, :] < order[:, None]).astype(jnp.bfloat16)
    earlier = jnp.dot(before, onehot.astype(jnp.bfloat16), preferred_element_type=jnp.float32)
    within = jnp.sum(jnp.where(onehot, earlier, 0.0), axis=1).astype(jnp.int32)
    return (flat_routes * capacity + within).reshape(row_count, top_count)


MESH = pl.DeviceIdType.MESH


def greet(ep_count, tp_count, e, t):
    barrier = pltpu.get_barrier_semaphore()
    peers = 0
    for d in range(1, ep_count):
        pl.semaphore_signal(
            barrier, inc=1, device_id={"ep": lax.rem(e + d, ep_count)}, device_id_type=MESH
        )
        peers += 1
    pair = t // 2
    core = lax.rem(t, 2)
    for k in range(1, tp_count // 2):
        pl.semaphore_signal(
            barrier,
            inc=1,
            device_id={"tp": lax.rem(pair + k, tp_count // 2) * 2 + core},
            device_id_type=MESH,
        )
        peers += 1
    pl.semaphore_signal(
        barrier, inc=1, device_id={"tp": pair * 2 + 1 - core}, device_id_type=MESH
    )
    peers += 1
    pl.semaphore_wait(barrier, peers)


def remote(src, dst, send, recv, device):
    return pltpu.make_async_remote_copy(
        src_ref=src,
        dst_ref=dst,
        send_sem=send,
        recv_sem=recv,
        device_id=device,
        device_id_type=MESH,
    )


def whole_kernel(
    ep_count,
    tp_count,
    blocks,
    normed,
    kv,
    query,
    out_weight_hbm,
    gate_hbm,
    up_hbm,
    down_hbm,
    shared_gate_hbm,
    shared_up_hbm,
    shared_down_hbm,
    returned,
    shared_sum,
    mixed_sum,
    arrived,
    normed_all,
    kv_all,
    out_weight,
    gate,
    up,
    down,
    shared_gate,
    shared_up,
    shared_down,
    heads_scr,
    routed,
    shared,
    mixed,
    routed_pair,
    routed_out,
    routed_in,
    routed_done,
    shared_pair,
    shared_out,
    shared_in,
    mixed_pair,
    mixed_out,
    mixed_in,
    local_sem,
    kv_send,
    kv_recv,
    z_send,
    z_recv,
    x_send,
    x_recv,
    d_send,
    d_recv,
    back_d_send,
    back_d_recv,
    back_x_send,
    back_x_recv,
    back_z_send,
    back_z_recv,
):
    e = lax.axis_index("ep")
    t = lax.axis_index("tp")
    half = tp_count // 2
    pair = t // 2
    core = lax.rem(t, 2)
    sibling = {"tp": pair * 2 + 1 - core}
    f32 = jnp.float32
    bf16 = jnp.bfloat16
    loads = [
        pltpu.make_async_copy(source, target, local_sem.at[3 + n])
        for n, (source, target) in enumerate(
            (
                (out_weight_hbm, out_weight),
                (gate_hbm, gate),
                (up_hbm, up),
                (down_hbm, down),
                (shared_gate_hbm, shared_gate),
                (shared_up_hbm, shared_up),
                (shared_down_hbm, shared_down),
            )
        )
    ]
    for copy in loads:
        copy.start()
    greet(ep_count, tp_count, e, t)

    sends = []

    def send(src, dst, send_sem, recv_sem, device):
        copy = remote(src, dst, send_sem, recv_sem, device)
        copy.start()
        sends.append(copy)

    def landed(spot, recv_sem):
        remote(spot, spot, kv_send.at[0], recv_sem, sibling).wait_recv()

    def source_of(d):
        return lax.rem(e - d + ep_count, ep_count)

    def place(d, row):
        if d == ep_count:
            return normed_all.at[row]
        return arrived.at[:, row, source_of(d)]

    for d in range(1, ep_count):
        there = lax.rem(e + d, ep_count)
        send(kv, kv_all.at[e], kv_send.at[d], kv_recv.at[e], {"ep": there})
    for d in range(1, ep_count):
        there = lax.rem(e + d, ep_count)
        send(blocks.at[there], arrived.at[:, t, e], z_send.at[d], z_recv.at[e], {"ep": there})

    def spread(src, d):
        for k in range(1, half):
            other = lax.rem(pair + k, half)
            send(
                src,
                place(d, t),
                x_send.at[k, d],
                x_recv.at[pair, d],
                {"tp": other * 2 + core},
            )
        send(src, place(d, t), d_send.at[0, d], d_recv.at[pair, d], sibling)

    def pass_on(d):
        for k in range(1, half):
            other = lax.rem(pair + k, half)
            spot = place(d, other * 2 + core)
            landed(spot, x_recv.at[other, d])
            send(spot, spot, d_send.at[k, d], d_recv.at[other, d], sibling)

    def come(d):
        spot = arrived.at[:, t, source_of(d)]
        landed(spot, z_recv.at[source_of(d)])
        spread(spot, d)

    def all_here(d):
        for other in range(half):
            landed(place(d, other * 2 + 1 - core), d_recv.at[other, d])

    spread(blocks.at[e], 0)
    spread(normed, ep_count)
    own = [
        pltpu.make_async_copy(blocks.at[e], arrived.at[:, t, e], local_sem.at[0]),
        pltpu.make_async_copy(normed, normed_all.at[t], local_sem.at[1]),
        pltpu.make_async_copy(kv, kv_all.at[e], local_sem.at[2]),
    ]
    for copy in own:
        copy.start()

    query_rows, wide = query.shape[1], query.shape[2]
    model_width = normed.shape[1]
    tile = min(512, model_width)

    def attend(h):
        def step(b, carried):
            top_now, total_now, acc_now = carried
            block = kv_all[b]
            scores = lax.dot_general(
                query[h], block, (((1,), (1,)), ((), ())), preferred_element_type=f32
            )
            top_new = jnp.maximum(top_now, jnp.max(scores, axis=-1, keepdims=True))
            shrink = jnp.exp(top_now - top_new)
            exps = jnp.exp(scores - top_new)
            total_new = total_now * shrink + jnp.sum(exps, axis=-1, keepdims=True)
            acc_new = acc_now * shrink + jnp.dot(
                exps.astype(bf16), block, preferred_element_type=f32
            )
            return (top_new, total_new, acc_new)

        start = (
            jnp.full((query_rows, 1), -1e30, f32),
            jnp.zeros((query_rows, 1), f32),
            jnp.zeros((query_rows, wide), f32),
        )
        top, total, acc = lax.fori_loop(0, ep_count, step, start)
        return acc / total

    def attend_two(n):
        low = pltpu.roll(attend(2 * n), wide // 2, 1)
        high = attend(2 * n + 1)
        lane = lax.broadcasted_iota(jnp.int32, low.shape, 1)
        heads_scr[:, n * wide : (n + 1) * wide] = jnp.where(lane < wide // 2, low, high).astype(
            bf16
        )

    def project():
        def step(n, ignored):
            columns = pl.ds(pl.multiple_of(n * tile, tile), tile)
            part = jnp.dot(heads_scr[...], out_weight[:, columns], preferred_element_type=f32)
            mixed[:, :, columns] = part.astype(bf16).reshape(
                tp_count, query_rows // tp_count, tile
            )
            return ignored

        lax.fori_loop(0, model_width // tile, step, 0)

    def share():
        def step(row, ignored):
            rows = normed_all[row]
            gate_part = jnp.dot(rows, shared_gate[...], preferred_element_type=f32)
            up_part = jnp.dot(rows, shared_up[...], preferred_element_type=f32)
            hidden = (gate_part / (1.0 + jnp.exp(-gate_part)) * up_part).astype(bf16)
            shared[row] = jnp.dot(hidden, shared_down[...], preferred_element_type=f32).astype(
                bf16
            )
            return ignored

        lax.fori_loop(0, tp_count, step, 0)

    local_count, capacity = arrived.shape[0], arrived.shape[3]

    def experts(d):
        source = source_of(d)

        def step(n, ignored):
            rows = arrived[n, :, source]
            if capacity % 16:
                rows = rows.astype(f32)
            rows = rows.reshape(tp_count * capacity, model_width).astype(bf16)
            gate_part = jnp.dot(rows, gate[n], preferred_element_type=f32)
            up_part = jnp.dot(rows, up[n], preferred_element_type=f32)
            hidden = (gate_part / (1.0 + jnp.exp(-gate_part)) * up_part).astype(bf16)

            def columns_step(m, inner):
                columns = pl.ds(pl.multiple_of(m * tile, tile), tile)
                part = jnp.dot(hidden, down[n, :, columns], preferred_element_type=f32)
                if capacity % 16:
                    part = part.reshape(tp_count, capacity, tile).astype(bf16)
                else:
                    part = part.astype(bf16).reshape(tp_count, capacity, tile)
                routed[n, :, source, :, columns] = part
                return inner

            lax.fori_loop(0, model_width // tile, columns_step, 0)
            return ignored

        lax.fori_loop(0, local_count, step, 0)

    def item(d):
        if d < ep_count:
            source = source_of(d)
            return (
                lambda row: routed.at[:, row, source],
                lambda k: routed_pair.at[d, k],
                lambda k: routed_out.at[d, k - 1],
                lambda k: routed_in.at[d, k - 1],
            )
        if d == ep_count:
            return (
                lambda row: shared.at[row],
                lambda k: shared_pair.at[k],
                lambda k: shared_out.at[k - 1],
                lambda k: shared_in.at[k - 1],
            )
        return (
            lambda row: mixed.at[row],
            lambda k: mixed_pair.at[k],
            lambda k: mixed_out.at[k - 1],
            lambda k: mixed_in.at[k - 1],
        )

    def to_sibling(d):
        part, paired, out, into = item(d)
        for k in list(range(1, half)) + [0]:
            other = lax.rem(pair + k, half)
            send(
                part(other * 2 + 1 - core),
                paired(k),
                back_d_send.at[d, k],
                back_d_recv.at[d, k],
                sibling,
            )

    def both(d, k):
        part, paired, out, into = item(d)
        spot = paired(k)
        landed(spot, back_d_recv.at[d, k])
        mine = part(lax.rem(pair + k, half) * 2 + core)
        return mine[...].astype(f32) + spot[...].astype(f32)

    crossed = set()

    def across(d):
        if d in crossed:
            return
        crossed.add(d)
        part, paired, out, into = item(d)
        for k in range(1, half):
            other = lax.rem(pair + k, half)
            out(k)[...] = both(d, k).astype(bf16)
            send(
                out(k),
                into(k),
                back_x_send.at[d, k],
                back_x_recv.at[d, k],
                {"tp": other * 2 + core},
            )

    finished = set()

    def finish(d):
        if d in finished:
            return
        finished.add(d)
        part, paired, out, into = item(d)
        total = both(d, 0)
        for k in range(1, half):
            spot = into(k)
            landed(spot, back_x_recv.at[d, k])
            total = total + spot[...].astype(f32)
        if d == 0:
            returned[e] = total.astype(bf16)
        elif d < ep_count:
            routed_done[d] = total.astype(bf16)
            send(
                routed_done.at[d],
                returned.at[e],
                back_z_send.at[d],
                back_z_recv.at[e],
                {"ep": source_of(d)},
            )
        elif d == ep_count:
            shared_sum[...] = total
        else:
            mixed_sum[...] = total.astype(bf16)

    last = ep_count - 1
    own[2].wait()
    for d in range(1, ep_count):
        landed(kv_all.at[source_of(d)], kv_recv.at[source_of(d)])
    pair_count = query.shape[0] // 2
    for n in range(pair_count):
        attend_two(n)
        if n == 0:
            pass_on(0)
    pass_on(ep_count)
    loads[0].wait()

    def expert_item(d):
        all_here(d)
        if d == 0:
            own[0].wait()
            for copy in loads[1:]:
                copy.wait()
        experts(d)
        to_sibling(d)

    for d in range(1, ep_count):
        come(d)
        if d == 1:
            project()
            to_sibling(ep_count + 1)
        else:
            pass_on(d - 1)
            expert_item(d - 2)
            if d == 2:
                all_here(ep_count)
                own[1].wait()
                share()
                to_sibling(ep_count)
            if d - 3 >= 1:
                across(d - 3)
    for d in range(1, last - 1):
        across(d)
    expert_item(last - 1)
    pass_on(last)
    across(last - 1)
    expert_item(last)
    for d in range(1, last - 1):
        finish(d)
    across(last)
    across(0)
    across(ep_count)
    across(ep_count + 1)
    for d in list(range(1, ep_count)) + [0, ep_count, ep_count + 1]:
        finish(d)
    for d in range(1, ep_count):
        landed(returned.at[source_of(d)], back_z_recv.at[source_of(d)])
    for copy in sends:
        copy.wait_send()


def whole(ep_count, tp_count, blocks, normed, kv, query, weights):
    local_count, capacity, width = blocks.shape[1:]
    vmem = pl.BlockSpec(memory_space=pltpu.VMEM)
    anywhere = pl.BlockSpec(memory_space=pl.ANY)
    half = tp_count // 2
    dma = pltpu.SemaphoreType.DMA
    block = (local_count, capacity, width)
    spread_block = (local_count, tp_count, ep_count, capacity, width)
    mixed = (query.shape[1] // tp_count, width)
    count = ep_count + 2

    def room(*shape):
        return pltpu.VMEM(shape, jnp.bfloat16)

    return pl.pallas_call(
        functools.partial(whole_kernel, ep_count, tp_count),
        out_shape=(
            jax.ShapeDtypeStruct((ep_count,) + block, jnp.bfloat16),
            jax.ShapeDtypeStruct(normed.shape, jnp.float32),
            jax.ShapeDtypeStruct(mixed, jnp.bfloat16),
        ),
        in_specs=[vmem] * 4 + [anywhere] * len(weights),
        out_specs=(vmem,) * 3,
        scratch_shapes=[
            room(*spread_block),
            room(tp_count, *normed.shape),
            room(ep_count, *kv.shape),
            *[room(*w.shape) for w in weights],
            room(query.shape[1], query.shape[0] // 2 * query.shape[2]),
            room(*spread_block),
            room(tp_count, *normed.shape),
            room(tp_count, *mixed),
            room(ep_count, half, *block),
            room(ep_count, half - 1, *block),
            room(ep_count, half - 1, *block),
            room(ep_count, *block),
            room(half, *normed.shape),
            room(half - 1, *normed.shape),
            room(half - 1, *normed.shape),
            room(half, *mixed),
            room(half - 1, *mixed),
            room(half - 1, *mixed),
            dma((3 + len(weights),)),
            dma((ep_count,)),
            dma((ep_count,)),
            dma((ep_count,)),
            dma((ep_count,)),
            dma((half, ep_count + 1)),
            dma((half, ep_count + 1)),
            dma((half, ep_count + 1)),
            dma((half, ep_count + 1)),
            dma((count, half)),
            dma((count, half)),
            dma((count, half)),
            dma((count, half)),
            dma((ep_count,)),
            dma((ep_count,)),
        ],
        compiler_params=pltpu.CompilerParams(
            collective_id=0, has_side_effects=True, vmem_limit_bytes=67043328
        ),
    )(blocks, normed, kv, query, *weights)


def body(
    queries,
    key_values,
    query_gain,
    key_gain,
    out_weight,
    second_batch,
    norm_gain,
    routes,
    route_weights,
    expert_gate,
    expert_up,
    expert_down,
    shared_gate,
    shared_up,
    shared_down,
):
    query_rows = queries.shape[0]
    head_size = query_gain.shape[0]
    heads_here = queries.shape[1] // head_size
    ep_count = lax.axis_size("ep")
    tp_count = lax.axis_size("tp")
    positions = lax.axis_index("ep") * query_rows + jnp.arange(query_rows, dtype=jnp.int32)
    query_turned = (
        turn_heads(
            head_norm(
                queries.reshape(query_rows, heads_here, head_size).astype(jnp.float32), query_gain
            ),
            positions,
        )
        * head_size ** (-0.5)
    ).astype(jnp.bfloat16)
    key_turned = turn_heads(
        head_norm(key_values[:, None, :head_size].astype(jnp.float32), key_gain), positions
    ).astype(jnp.bfloat16)
    keys_and_values = jnp.concatenate([key_turned[:, 0, :], key_values[:, head_size:]], axis=1)
    tok_count = second_batch.shape[0]
    model_width = second_batch.shape[1]
    top_count = routes.shape[1]
    local_experts = expert_gate.shape[0]
    expert_count = local_experts * ep_count
    capacity = 3 * tok_count * top_count // (2 * expert_count)
    capacity = (capacity + 7) // 8 * 8
    slot_count = expert_count * capacity
    token_float = second_batch.astype(jnp.float32)
    normed = (
        token_float
        * lax.rsqrt(jnp.mean(token_float * token_float, axis=-1, keepdims=True) + norm_eps)
        * norm_gain
    ).astype(jnp.bfloat16)
    own_slots = slot_ids(routes, expert_count, capacity)
    slot_numbers = jnp.arange(slot_count, dtype=jnp.int32)
    picks = [
        (own_slots[:, j][:, None] == slot_numbers[None, :]).astype(jnp.bfloat16)
        for j in range(top_count)
    ]
    outgoing = lax.dot_general(
        sum(picks), normed, (((0,), (0,)), ((), ())), preferred_element_type=jnp.float32
    ).astype(jnp.bfloat16)
    query_wide = jnp.pad(
        query_turned.transpose(1, 0, 2), ((0, 0), (0, 0), (0, key_values.shape[1] - head_size))
    )
    returned, shared_sum, mixer_out = whole(
        ep_count,
        tp_count,
        outgoing.reshape(ep_count, local_experts, capacity, model_width),
        normed,
        keys_and_values,
        query_wide,
        (
            out_weight,
            expert_gate,
            expert_up,
            expert_down,
            shared_gate,
            shared_up,
            shared_down,
        ),
    )
    returned = returned.reshape(slot_count, model_width)
    combined = shared_sum
    for j in range(top_count):
        combined = combined + route_weights[:, j : j + 1] * jnp.dot(
            picks[j], returned, preferred_element_type=jnp.float32
        )
    return (mixer_out, combined.astype(jnp.bfloat16))


def solution(mesh):
    placed = (
        P(("grp", "ep"), "tp"),
        P(("grp", "ep"), "tp"),
        P(),
        P(),
        P("tp", None),
        P(("grp", "ep", "tp"), None),
        P(),
        P(("grp", "ep", "tp"), None),
        P(("grp", "ep", "tp"), None),
        P("ep", None, "tp"),
        P("ep", None, "tp"),
        P("ep", "tp", None),
        P(None, "tp"),
        P(None, "tp"),
        P("tp", None),
    )
    return jax.shard_map(
        body,
        mesh=mesh,
        in_specs=placed,
        out_specs=(P(("grp", "ep", "tp"), None), P(("grp", "ep", "tp"), None)),
        check_vma=False,
    )
```

time: 294 us -> 138 us (0.47)
  the two profiles are of different devices: /device:TPU:0 before, /device:TPU:8 now
where the time goes in v2:
time: 138 us
  Pallas kernels  123 us (89%)
  local copies, waits for them, and re-layouts  6.68 us (5%)
  matrix products  5.62 us (4%)
  other arithmetic  2.01 us (1%)
    pallas_call x1, Pallas kernels, whole(): pl.pallas_call(functools.partial(whole_kernel, ep_count, tp_count), out_s...  123 us
    dot_general x2, matrix products, body(): jnp.dot(picks[j], returned, preferred_element_type=jnp.float32)  3.6 us
    unnamed x26, local copies, waits for them, and re-layouts  2.89 us

profile of v2, /device:TPU:8, one launch (start us, length us, event | category | flops | bytes accessed | tf_op | source)
XLA Modules:
  0.0 138.1 jit_solution(7100347525515513380)
XLA Ops:
  0.7 0.2 fusion.21
  0.9 1.1 copy.44
  2.0 0.2 reshape.338
  2.3 0.8 mul.261
  3.1 0.1 fusion.8
  3.4 0.2 copy.47
  3.5 0.3 copy.48
  3.8 0.8 pad.4.query
  5.2 0.2 subtract_convert_fusion
  5.5 0.1 copy.43
  5.6 0.7 pad_maximum_fusion.kv
  6.3 0.1 copy.37
  6.4 0.1 eq.48
  6.6 0.2 fusion.3
  6.8 0.1 convert_element_type.73
  7.1 0.2 fusion.4
  7.3 0.2 fusion.6.normed
  7.5 0.8 copy-done.1
  8.3 1.8 %convolution_convert_fusion = bf16[384,2048]{1,0:T(8,128)(2,1)} fusion(bf16[128,2048]{1,0:T(8,128)(2,1)S(1)} %fusion.6.normed, s32[128]{0:T(128)S(1)} %get-tuple-element.25, s32[128]{0:T(128)S(1)} %get-tuple-element.24), kind=kOutput, calls=%fused_computation | convolution fusion | flops 202506240 | bytes 2098176 | tf_op jit(solution)/shard_map/dot_general | solution.py:589
  10.1 122.9 %shard_map.158 = (bf16[4,2,48,2048]{3,2,1,0:T(8,128)(2,1)}, f32[128,2048]{1,0:T(8,128)}, bf16[96,2048]{1,0:T(8,128)(2,1)}) custom-call(bf16[4,2,48,2048]{3,2,1,0:T(8,128)(2,1)} %bitcast.29, bf16[128,2048]{1,0:T(8,128)(2,1)} %copy-done.1, bf16[384,128]{1,0:T(8,128)(2,1)} %pad_maximum_fusion.kv, bf16[4,384,128]{2,1,0:T(8,128)(2,1)} %pad.4.query, ...), custom_call_target="tpu_custom_call" | custom-call | tf_op jit(solution)/shard_map/pallas_call | solution.py:483
  132.9 0.8 slice_bitcast_fusion
  133.7 2.3 %fusion.1 = f32[128,2048]{1,0:T(8,128)S(1)} fusion(f32[128,2048]{1,0:T(8,128)} %get-tuple-element.6, bf16[384,2048]{1,0:T(8,128)(2,1)} %bitcast.27, f32[128]{0:T(128)S(1)} %get-tuple-element.23, s32[128]{0:T(128)} %copy-done.8), kind=kOutput, calls=%fused_computation.4 | convolution fusion | flops 201900032 | bytes 3671040 | tf_op jit(solution)/shard_map/dot_general | solution.py:615
  136.1 1.3 fusion.2
  137.4 0.7 copy.60
  (44 shorter events, 1.0 us)
Async XLA Ops:
  3.3 1.4 %copy-start.4 = (bf16[384,128]{1,0:T(8,128)(2,1)S(1)}, bf16[384,128]{1,0:T(8,128)(2,1)}, u32[]{:S(2)}) copy-start(bf16[384,128]{1,0:T(8,128)(2,1)} %param.16) | copy-start | bytes 294916
  3.3 1.6 %copy-start.10 = (f32[64]{0:T(128)S(1)}, f32[64]{0:T(128)}, u32[]{:S(2)}) copy-start(f32[64]{0:T(128)} %param.18) | copy-start | bytes 772
  3.8 2.5 %copy-start.9 = (s32[128,2]{0,1:T(2,128)S(1)}, s32[128,2]{0,1:T(2,128)}, u32[]{:S(2)}) copy-start(s32[128,2]{0,1:T(2,128)} %param.22) | copy-start | bytes 3076
  3.8 3.2 %copy-start.2 = (bf16[128,2048]{1,0:T(8,128)(2,1)S(1)}, bf16[128,2048]{1,0:T(8,128)(2,1)}, u32[]{:S(2)}) copy-start(bf16[128,2048]{1,0:T(8,128)(2,1)} %param.20) | copy-start | bytes 1572868
  4.7 2.6 %copy-start.5 = (f32[2048]{0:T(1024)S(1)}, f32[2048]{0:T(1024)}, u32[]{:S(2)}) copy-start(f32[2048]{0:T(1024)} %param.21) | copy-start | bytes 24580
  7.0 3.1 %copy-start.6 = (s32[128]{0:T(128)}, s32[128]{0:T(128)S(1)}, u32[]{:S(2)}) copy-start(s32[128]{0:T(128)S(1)} %get-tuple-element.25) | copy-start | bytes 1540
  7.0 3.0 %copy-start.8 = (s32[128]{0:T(128)}, s32[128]{0:T(128)S(1)}, u32[]{:S(2)}) copy-start(s32[128]{0:T(128)S(1)} %get-tuple-element.24) | copy-start | bytes 1540
  7.5 0.8 copy-start.1
  133.7 2.3 %copy-start = (bf16[4,2,48,2048]{3,2,1,0:T(8,128)(2,1)S(1)}, bf16[4,2,48,2048]{3,2,1,0:T(8,128)(2,1)}, u32[]{:S(2)}) copy-start(bf16[4,2,48,2048]{3,2,1,0:T(8,128)(2,1)} %get-tuple-element.7) | copy-start | bytes 4718596
  133.7 2.3 %copy-start.7 = (s32[128]{0:T(128)S(1)}, s32[128]{0:T(128)}, u32[]{:S(2)}) copy-start(s32[128]{0:T(128)} %copy-done.6) | copy-start | bytes 1540
  136.0 1.3 copy-start.3

commit v3 on v2

--- a/solution.py
+++ b/solution.py
@@ -94,6 +94,7 @@
     normed,
     kv,
     query,
+    picking,
     out_weight_hbm,
     gate_hbm,
     up_hbm,
@@ -107,6 +108,7 @@
     arrived,
     normed_all,
     kv_all,
+    picking_all,
     out_weight,
     gate,
     up,
@@ -186,6 +188,8 @@
     def place(d, row):
         if d == ep_count:
             return normed_all.at[row]
+        if d == ep_count + 1:
+            return picking_all.at[row]
         return arrived.at[:, row, source_of(d)]
 
     for d in range(1, ep_count):
@@ -223,10 +227,10 @@
         for other in range(half):
             landed(place(d, other * 2 + 1 - core), d_recv.at[other, d])
 
-    spread(blocks.at[e], 0)
+    spread(picking, ep_count + 1)
     spread(normed, ep_count)
     own = [
-        pltpu.make_async_copy(blocks.at[e], arrived.at[:, t, e], local_sem.at[0]),
+        pltpu.make_async_copy(picking, picking_all.at[t], local_sem.at[0]),
         pltpu.make_async_copy(normed, normed_all.at[t], local_sem.at[1]),
         pltpu.make_async_copy(kv, kv_all.at[e], local_sem.at[2]),
     ]
@@ -280,20 +284,56 @@
 
         lax.fori_loop(0, model_width // tile, step, 0)
 
+    local_count, capacity = arrived.shape[0], arrived.shape[3]
+
     def share():
         def step(row, ignored):
             rows = normed_all[row]
             gate_part = jnp.dot(rows, shared_gate[...], preferred_element_type=f32)
             up_part = jnp.dot(rows, shared_up[...], preferred_element_type=f32)
             hidden = (gate_part / (1.0 + jnp.exp(-gate_part)) * up_part).astype(bf16)
-            shared[row] = jnp.dot(hidden, shared_down[...], preferred_element_type=f32).astype(
-                bf16
-            )
+            weight = picking_all[row, 1]
+            weight_high = weight.astype(bf16)
+            weight_low = (weight - weight_high.astype(f32)).astype(bf16)
+
+            def columns_step(m, inner):
+                columns = pl.ds(pl.multiple_of(m * tile, tile), tile)
+                results = routed[:, row, e, :, columns]
+                if capacity % 16:
+                    results = results.astype(f32)
+                results = results.reshape(local_count * capacity, tile).astype(bf16)
+                part = jnp.dot(hidden, shared_down[:, columns], preferred_element_type=f32)
+                part = part + jnp.dot(weight_high, results, preferred_element_type=f32)
+                part = part + jnp.dot(weight_low, results, preferred_element_type=f32)
+                shared[row, :, columns] = part.astype(bf16)
+                return inner
+
+            lax.fori_loop(0, model_width // tile, columns_step, 0)
             return ignored
 
         lax.fori_loop(0, tp_count, step, 0)
 
-    local_count, capacity = arrived.shape[0], arrived.shape[3]
+    def pick_own():
+        def step(row, ignored):
+            chosen = picking_all[row, 0].astype(bf16)
+
+            def columns_step(m, inner):
+                columns = pl.ds(pl.multiple_of(m * tile, tile), tile)
+                part = lax.dot_general(
+                    chosen,
+                    normed_all[row, :, columns],
+                    (((0,), (0,)), ((), ())),
+                    preferred_element_type=f32,
+                )
+                arrived[:, row, e, :, columns] = part.reshape(local_count, capacity, tile).astype(
+                    bf16
+                )
+                return inner
+
+            lax.fori_loop(0, model_width // tile, columns_step, 0)
+            return ignored
+
+        lax.fori_loop(0, tp_count, step, 0)
 
     def experts(d):
         source = source_of(d)
@@ -394,9 +434,7 @@
             spot = into(k)
             landed(spot, back_x_recv.at[d, k])
             total = total + spot[...].astype(f32)
-        if d == 0:
-            returned[e] = total.astype(bf16)
-        elif d < ep_count:
+        if d < ep_count:
             routed_done[d] = total.astype(bf16)
             send(
                 routed_done.at[d],
@@ -417,17 +455,25 @@
     pair_count = query.shape[0] // 2
     for n in range(pair_count):
         attend_two(n)
-        if n == 0:
-            pass_on(0)
+    pass_on(ep_count + 1)
     pass_on(ep_count)
     loads[0].wait()
 
     def expert_item(d):
-        all_here(d)
         if d == 0:
+            all_here(ep_count + 1)
+            all_here(ep_count)
             own[0].wait()
+            own[1].wait()
+            pick_own()
             for copy in loads[1:]:
                 copy.wait()
+            experts(0)
+            share()
+            to_sibling(ep_count)
+            returned[e] = jnp.zeros(returned.shape[1:], bf16)
+            return
+        all_here(d)
         experts(d)
         to_sibling(d)
 
@@ -438,12 +484,9 @@
             to_sibling(ep_count + 1)
         else:
             pass_on(d - 1)
+            if d == 2:
+                across(ep_count + 1)
             expert_item(d - 2)
-            if d == 2:
-                all_here(ep_count)
-                own[1].wait()
-                share()
-                to_sibling(ep_count)
             if d - 3 >= 1:
                 across(d - 3)
     for d in range(1, last - 1):
@@ -455,10 +498,9 @@
     for d in range(1, last - 1):
         finish(d)
     across(last)
-    across(0)
     across(ep_count)
     across(ep_count + 1)
-    for d in list(range(1, ep_count)) + [0, ep_count, ep_count + 1]:
+    for d in list(range(1, ep_count)) + [ep_count, ep_count + 1]:
         finish(d)
     for d in range(1, ep_count):
         landed(returned.at[source_of(d)], back_z_recv.at[source_of(d)])
@@ -466,7 +508,7 @@
         copy.wait_send()
 
 
-def whole(ep_count, tp_count, blocks, normed, kv, query, weights):
+def whole(ep_count, tp_count, blocks, normed, kv, query, picking, weights):
     local_count, capacity, width = blocks.shape[1:]
     vmem = pl.BlockSpec(memory_space=pltpu.VMEM)
     anywhere = pl.BlockSpec(memory_space=pl.ANY)
@@ -487,12 +529,13 @@
             jax.ShapeDtypeStruct(normed.shape, jnp.float32),
             jax.ShapeDtypeStruct(mixed, jnp.bfloat16),
         ),
-        in_specs=[vmem] * 4 + [anywhere] * len(weights),
+        in_specs=[vmem] * 5 + [anywhere] * len(weights),
         out_specs=(vmem,) * 3,
         scratch_shapes=[
             room(*spread_block),
             room(tp_count, *normed.shape),
             room(ep_count, *kv.shape),
+            pltpu.VMEM((tp_count,) + picking.shape, jnp.float32),
             *[room(*w.shape) for w in weights],
             room(query.shape[1], query.shape[0] // 2 * query.shape[2]),
             room(*spread_block),
@@ -513,10 +556,10 @@
             dma((ep_count,)),
             dma((ep_count,)),
             dma((ep_count,)),
-            dma((half, ep_count + 1)),
-            dma((half, ep_count + 1)),
-            dma((half, ep_count + 1)),
-            dma((half, ep_count + 1)),
+            dma((half, ep_count + 2)),
+            dma((half, ep_count + 2)),
+            dma((half, ep_count + 2)),
+            dma((half, ep_count + 2)),
             dma((count, half)),
             dma((count, half)),
             dma((count, half)),
@@ -527,7 +570,7 @@
         compiler_params=pltpu.CompilerParams(
             collective_id=0, has_side_effects=True, vmem_limit_bytes=67043328
         ),
-    )(blocks, normed, kv, query, *weights)
+    )(blocks, normed, kv, query, picking, *weights)
 
 
 def body(
@@ -589,6 +632,17 @@
     outgoing = lax.dot_general(
         sum(picks), normed, (((0,), (0,)), ((), ())), preferred_element_type=jnp.float32
     ).astype(jnp.bfloat16)
+    near_count = local_experts * capacity
+    near_slots = lax.axis_index("ep") * near_count + jnp.arange(near_count, dtype=jnp.int32)
+    near = [own_slots[:, j][:, None] == near_slots[None, :] for j in range(top_count)]
+    picking = jnp.stack(
+        [
+            sum(jnp.where(match, 1.0, 0.0) for match in near),
+            sum(
+                jnp.where(match, route_weights[:, j : j + 1], 0.0) for j, match in enumerate(near)
+            ),
+        ]
+    )
     query_wide = jnp.pad(
         query_turned.transpose(1, 0, 2), ((0, 0), (0, 0), (0, key_values.shape[1] - head_size))
     )
@@ -599,6 +653,7 @@
         normed,
         keys_and_values,
         query_wide,
+        picking,
         (
             out_weight,
             expert_gate,

time: 138 us -> 135 us (0.978)
  the two profiles are of different devices: /device:TPU:8 before, /device:TPU:0 now
where the time goes in v3:
time: 135 us
  Pallas kernels  118 us (87%)
  local copies, waits for them, and re-layouts  6.45 us (5%)
  matrix products  5.61 us (4%)
  other arithmetic  4.58 us (3%)
    pallas_call x1, Pallas kernels, whole(): pl.pallas_call(functools.partial(whole_kernel, ep_count, tp_count), out_s...  118 us
    dot_general x2, matrix products, body(): jnp.dot(picks[j], returned, preferred_element_type=jnp.float32)  3.59 us

profile of v3, /device:TPU:0, one launch (start us, length us, event | category | flops | bytes accessed | tf_op | source)
XLA Modules:
  0.0 135.1 jit_solution(8874780139936047709)
XLA Ops:
  0.7 1.3 fusion.4
  2.0 0.8 slice_bitcast_fusion.1
  2.7 0.8 mul.260
  3.6 0.8 copy.37
  4.4 0.1 eq.94
  4.5 0.2 fusion.3
  4.9 0.7 multiply_add_fusion.1
  5.7 0.2 fusion.23
  5.9 0.1 fusion.20
  6.1 0.7 pad_maximum_fusion.picking
  6.7 0.2 copy.44
  7.0 0.2 reshape.618
  7.4 0.2 copy.47
  7.6 0.3 copy.48
  7.9 0.8 pad.4.query
  9.2 0.2 subtract_convert_fusion
  9.6 0.7 pad_maximum_fusion.1.kv
  10.3 0.2 fusion.6.normed
  10.6 0.8 copy-done.1
  11.4 1.8 %convolution_convert_fusion = bf16[384,2048]{1,0:T(8,128)(2,1)} fusion(bf16[128,2048]{1,0:T(8,128)(2,1)S(1)} %fusion.6.normed, s32[128]{0:T(128)S(1)} %get-tuple-element.27, s32[128]{0:T(128)S(1)} %get-tuple-element.26), kind=kOutput, calls=%fused_computation | convolution fusion | flops 202506240 | bytes 2098176 | tf_op jit(solution)/shard_map/dot_general | solution.py:632
  13.2 117.5 %shard_map.158 = (bf16[4,2,48,2048]{3,2,1,0:T(8,128)(2,1)}, f32[128,2048]{1,0:T(8,128)}, bf16[96,2048]{1,0:T(8,128)(2,1)}) custom-call(bf16[4,2,48,2048]{3,2,1,0:T(8,128)(2,1)} %bitcast.29, bf16[128,2048]{1,0:T(8,128)(2,1)} %copy-done.1, bf16[384,128]{1,0:T(8,128)(2,1)} %pad_maximum_fusion.1.kv, bf16[4,384,128]{2,1,0:T(8,128)(2,1)} %pad.4.query, ...), custom_call_target="tpu_custom_call" | custom-call | tf_op jit(solution)/shard_map/pallas_call | solution.py:525
  130.7 2.3 %fusion.1 = f32[128,2048]{1,0:T(8,128)S(1)} fusion(f32[128,2048]{1,0:T(8,128)} %get-tuple-element.6, bf16[384,2048]{1,0:T(8,128)(2,1)} %bitcast.27, f32[128]{0:T(128)} %copy-done.12, s32[128]{0:T(128)} %copy-done.9), kind=kOutput, calls=%fused_computation.4 | convolution fusion | flops 201900032 | bytes 3671040 | tf_op jit(solution)/shard_map/dot_general | solution.py:670
  133.1 1.3 fusion.2
  134.4 0.7 copy.60
  (53 shorter events, 1.4 us)
Async XLA Ops:
  0.6 6.1 %copy-start.5 = (bf16[384,256]{1,0:T(8,128)(2,1)S(1)}, bf16[384,256]{1,0:T(8,128)(2,1)}, u32[]{:S(2)}) copy-start(bf16[384,256]{1,0:T(8,128)(2,1)} %param.15) | copy-start | bytes 589828
  2.7 3.3 %copy-start.10 = (f32[128]{0:T(128)}, f32[128]{0:T(128)S(1)}, u32[]{:S(2)}) copy-start(f32[128]{0:T(128)S(1)} %get-tuple-element.25) | copy-start | bytes 1540
  2.7 3.3 %copy-start.12 = (f32[128]{0:T(128)}, f32[128]{0:T(128)S(1)}, u32[]{:S(2)}) copy-start(f32[128]{0:T(128)S(1)} %get-tuple-element.24) | copy-start | bytes 1540
  5.6 4.9 %copy-start.7 = (s32[128]{0:T(128)}, s32[128]{0:T(128)S(1)}, u32[]{:S(2)}) copy-start(s32[128]{0:T(128)S(1)} %get-tuple-element.27) | copy-start | bytes 1540
  5.6 4.9 %copy-start.9 = (s32[128]{0:T(128)}, s32[128]{0:T(128)S(1)}, u32[]{:S(2)}) copy-start(s32[128]{0:T(128)S(1)} %get-tuple-element.26) | copy-start | bytes 1540
  7.3 1.4 %copy-start.4 = (bf16[384,128]{1,0:T(8,128)(2,1)S(1)}, bf16[384,128]{1,0:T(8,128)(2,1)}, u32[]{:S(2)}) copy-start(bf16[384,128]{1,0:T(8,128)(2,1)} %param.16) | copy-start | bytes 294916
  7.3 1.6 %copy-start.13 = (f32[64]{0:T(128)S(1)}, f32[64]{0:T(128)}, u32[]{:S(2)}) copy-start(f32[64]{0:T(128)} %param.18) | copy-start | bytes 772
  7.8 2.5 %copy-start.2 = (bf16[128,2048]{1,0:T(8,128)(2,1)S(1)}, bf16[128,2048]{1,0:T(8,128)(2,1)}, u32[]{:S(2)}) copy-start(bf16[128,2048]{1,0:T(8,128)(2,1)} %param.20) | copy-start | bytes 1572868
  7.9 2.5 %copy-start.6 = (f32[2048]{0:T(1024)S(1)}, f32[2048]{0:T(1024)}, u32[]{:S(2)}) copy-start(f32[2048]{0:T(1024)} %param.21) | copy-start | bytes 24580
  10.6 0.8 copy-start.1
  130.7 2.3 %copy-start = (bf16[4,2,48,2048]{3,2,1,0:T(8,128)(2,1)S(1)}, bf16[4,2,48,2048]{3,2,1,0:T(8,128)(2,1)}, u32[]{:S(2)}) copy-start(bf16[4,2,48,2048]{3,2,1,0:T(8,128)(2,1)} %get-tuple-element.7) | copy-start | bytes 4718596
  130.7 2.3 %copy-start.8 = (s32[128]{0:T(128)S(1)}, s32[128]{0:T(128)}, u32[]{:S(2)}) copy-start(s32[128]{0:T(128)} %copy-done.7) | copy-start | bytes 1540
  130.7 2.3 %copy-start.11 = (f32[128]{0:T(128)S(1)}, f32[128]{0:T(128)}, u32[]{:S(2)}) copy-start(f32[128]{0:T(128)} %copy-done.10) | copy-start | bytes 1540
  133.1 1.3 copy-start.3
